TPU v7x, 32 devices: a whole 2x2x4 slice. The times are simulated.
32 devices in a mesh: grp: 2 (over y), sp: 4 (over z), tp: 4 (over x, core).
Axes of the slice: x: 2, y: 2, z: 4, core: 2. Of those that a mesh axis runs over, the one named last changes fastest.
Arguments:
- query_rows: bfloat16 [1024, 1024], P(('grp', 'sp'), 'tp'), parts along dimension 0, may hold values from -6 to 6
- key_rows: bfloat16 [1024, 1024], P(('grp', 'sp'), 'tp'), parts along dimension 0, may hold values from -6 to 6
- value_rows: bfloat16 [1024, 1024], P(('grp', 'sp'), 'tp'), parts along dimension 0, may hold values from -6 to 6
- gate_rows: bfloat16 [1024, 1024], P(('grp', 'sp'), 'tp'), parts along dimension 0, may hold values from -6 to 6
- log_decay: float32 [2, 8, 1024], P(None, 'tp', ('grp', 'sp')), parts along dimension 2, may hold values from -2 to 0, as said below
- head_gain: float32 [2, 1024], P(None, 'tp'), may hold values from 0.1 to 1.9
- out_weight: bfloat16 [1024, 2048], P('tp'), may hold values from -0.1875 to 0.1875
- residual: bfloat16 [1024, 2048], P(('grp', 'sp')), parts along dimension 0, may hold values from -6 to 6
- norm_gain: bfloat16 [2048], replicated, may hold values from 0.099609375 to 1.8984375
- gate_weight: bfloat16 [2048, 5632], P('sp', 'tp'), may hold values from -0.125 to 0.125
- up_weight: bfloat16 [2048, 5632], P('sp', 'tp'), may hold values from -0.125 to 0.125
- down_weight: bfloat16 [2048, 5632], P('sp', 'tp'), may hold values from -0.078125 to 0.078125
- gate_taps: bfloat16 [3, 5632], P(None, 'tp'), may hold values from -3.5 to 3.5
- up_taps: bfloat16 [3, 5632], P(None, 'tp'), may hold values from -3.5 to 3.5
Outputs:
- block_out: bfloat16 [1024, 2048], P(('grp', 'sp', 'tp')), parts along dimension 0
There are 2 independent parts, one for each index of `grp`. A program takes and returns all parts, laid end to end along the dimension named above; an argument that names none is the same for every part. Nothing has to cross between parts.
Inputs may be any that keep to these rules, and one draw needn't show every extreme that they name: `log_decay`: every entry is negative.
All inputs are finite; a program needn't handle non-finite values.
Results may differ from a plain program's by a relative error of at most 0.017.
Values may be sent and summed in bfloat16 or wider, within the bound.
A program may use at most 64 MiB of HBM per device.

v0:
```python
import functools
import math

import jax
import jax.numpy as jnp
from jax import lax
from jax.experimental import pallas as pl
from jax.experimental.pallas import tpu as pltpu
from jax.sharding import PartitionSpec as P

HEAD = 128
PIECES = 12
EDGE = 16
FLIGHT = 2
HEADSTART = 2
SKEW = 2


FULL_PRECISION = lax.Precision.HIGHEST
GROUP_EPS = 1e-05
NORM_EPS = 1e-06


def prefix(value, axis, join, neutral, backward):
    count, mine = (lax.axis_size(axis), lax.axis_index(axis))
    pieces = jax.tree.map(lambda part: lax.all_gather(part, axis), value)
    if backward:
        pieces = jax.tree.map(lambda part: part[::-1], pieces)
        mine = count - 1 - mine
    running = jax.tree.map(
        lambda part, zero: jnp.full_like(part, 0) + jnp.asarray(zero, part.dtype), value, neutral
    )

    def lap(position, running):
        longer = join(running, jax.tree.map(lambda part: part[position], pieces))
        return jax.tree.map(lambda new, old: jnp.where(position < mine, new, old), longer, running)

    return lax.fori_loop(0, count - 1, lap, running)


def padded_2(shard, sides, width):
    for axis, dim in sides:
        size, length = (lax.axis_size(axis), shard.shape[dim])
        up = [(i, (i + 1) % size) for i in range(size - 1)]
        down = [(j, i) for i, j in up]
        last = lax.slice_in_dim(shard, length - width, length, axis=dim)
        initial = lax.slice_in_dim(shard, 0, width, axis=dim)
        before = lax.ppermute(last, axis, up)
        after = lax.ppermute(initial, axis, down)
        shard = jnp.concatenate([before, shard, after], axis=dim)
    return shard


def state_combine(earlier, later):
    return (earlier[0] * later[0], earlier[1] * later[0][:, None, None] + later[1])


def group_norm(values):
    length, head_count, head_width = values.shape
    centre = values - jnp.mean(values, axis=2, keepdims=True)
    spread = jnp.mean(centre * centre, axis=2, keepdims=True)
    return (centre * lax.rsqrt(spread + GROUP_EPS)).reshape(length, head_count * head_width)


def rms_scale(middle, gain):
    values = middle.astype(jnp.float32)
    multiplier = lax.rsqrt(jnp.mean(values * values, axis=1, keepdims=True) + NORM_EPS)
    return (values * multiplier * gain.astype(jnp.float32)).astype(jnp.bfloat16)


def local_retention(query_all, key_all, value_all, log_rates):
    length, head_count, head_width = query_all.shape
    block_len = math.gcd(length, 512)
    block_count = length // block_len
    cumul = jnp.cumsum(log_rates, axis=1).T
    query_block = query_all.reshape(block_count, block_len, head_count, head_width)
    key_block = key_all.reshape(block_count, block_len, head_count, head_width)
    value_block = value_all.reshape(block_count, block_len, head_count, head_width)
    cumul_block = cumul.reshape(block_count, block_len, head_count)
    before = jnp.concatenate(
        [jnp.zeros((1, head_count), jnp.float32), cumul_block[:-1, -1]], axis=0
    )
    local_cumul = cumul_block - before[:, None, :]
    gap_logs = local_cumul[:, :, None, :] - local_cumul[:, None, :, :]
    lower_mask = (jnp.arange(block_len)[:, None] >= jnp.arange(block_len)[None, :])[
        None, :, :, None
    ]
    decay_mask = jnp.where(lower_mask, jnp.exp(jnp.minimum(gap_logs, 0.0)), 0.0)
    scores = (
        jnp.einsum("bthd,bshd->btsh", query_block, key_block, precision=FULL_PRECISION) * decay_mask
    )
    inner_part = jnp.einsum("btsh,bshe->bthe", scores, value_block, precision=FULL_PRECISION)
    to_end = jnp.exp(local_cumul[:, -1:, :] - local_cumul)
    block_states = jnp.einsum(
        "bshd,bshe->bhde", key_block * to_end[..., None], value_block, precision=FULL_PRECISION
    )
    block_decay = jnp.exp(local_cumul[:, -1, :])

    def carry_step(carry_state, inputs):
        return (carry_state * inputs[0][:, None, None] + inputs[1], carry_state)

    zero_state = jnp.zeros((head_count, head_width, head_width), jnp.float32)
    end_state, entering = lax.scan(carry_step, zero_state, (block_decay, block_states))
    carried = jnp.einsum(
        "bthd,bhde->bthe",
        query_block * jnp.exp(local_cumul)[..., None],
        entering,
        precision=FULL_PRECISION,
    )
    output = (inner_part + carried).reshape(length, head_count, head_width)
    return (output, end_state, cumul, jnp.exp(cumul[-1]))


def with_incoming(output, query_all, cumul, incoming):
    return output + jnp.einsum(
        "thd,hde->the", query_all * jnp.exp(cumul)[:, :, None], incoming, precision=FULL_PRECISION
    )


def shards(
    query_rows,
    key_rows,
    value_rows,
    gate_rows,
    log_decay,
    head_gain,
    out_weight,
    residual,
    norm_gain,
    gate_weight,
    up_weight,
    down_weight,
    gate_taps,
    up_taps,
):
    pair_local = jnp.concatenate([gate_weight, up_weight], axis=1)
    row_count = query_rows.shape[0]
    head_count = query_rows.shape[1] // HEAD
    key_scale = HEAD ** (-0.5)
    query_all = query_rows.astype(jnp.float32).reshape(row_count, head_count, HEAD)
    key_all = key_rows.astype(jnp.float32).reshape(row_count, head_count, HEAD) * key_scale
    value_all = value_rows.astype(jnp.float32).reshape(row_count, head_count, HEAD)
    identity = (
        jnp.ones((head_count,), jnp.float32),
        jnp.zeros((head_count, HEAD, HEAD), jnp.float32),
    )
    ahead_local, ahead_state, ahead_cumul, ahead_decay = local_retention(
        query_all, key_all, value_all, log_decay[0]
    )
    query_back = query_all[::-1]
    behind_local, behind_state, behind_cumul, behind_decay = local_retention(
        query_back, key_all[::-1], value_all[::-1], log_decay[1][:, ::-1]
    )
    ahead_in = prefix((ahead_decay, ahead_state), "sp", state_combine, identity, False)[1]
    behind_in = prefix((behind_decay, behind_state), "sp", state_combine, identity, True)[1]
    ahead_out = with_incoming(ahead_local, query_all, ahead_cumul, ahead_in)
    behind_out = with_incoming(behind_local, query_back, behind_cumul, behind_in)[::-1]
    combined = group_norm(ahead_out) * head_gain[0] + group_norm(behind_out) * head_gain[1]
    mixed_heads = (jax.nn.silu(gate_rows.astype(jnp.float32)) * combined).astype(jnp.bfloat16)
    gathered = (
        lax.all_gather(pair_local, "sp", axis=0, tiled=True),
        lax.all_gather(down_weight, "sp", axis=0, tiled=True),
    )
    pair_full, down_full = gathered
    share_rows = row_count // lax.axis_size("tp")
    own_start = lax.axis_index("tp") * share_rows
    picked = mixed_heads
    attended = lax.psum_scatter(
        jnp.dot(picked, out_weight, preferred_element_type=jnp.float32).astype(jnp.bfloat16),
        "tp",
        scatter_dimension=0,
        tiled=True,
    ).astype(jnp.float32)
    residual_own = lax.dynamic_slice_in_dim(residual, own_start, share_rows, 0)
    middle_own = lax.optimization_barrier(
        (residual_own.astype(jnp.float32) + attended).astype(jnp.bfloat16)
    )
    normed = rms_scale(middle_own, norm_gain)
    pre_both = jnp.dot(
        lax.all_gather(normed, "tp", axis=0, tiled=True),
        pair_full,
        preferred_element_type=jnp.float32,
    ).astype(jnp.bfloat16)
    padded = padded_2(pre_both, (("sp", 0),), 1)
    half_width = gate_taps.shape[1]
    tap_table = jnp.concatenate([gate_taps, up_taps], axis=1).astype(jnp.float32)
    conv_out = (
        tap_table[0] * padded[:-2].astype(jnp.float32)
        + tap_table[1] * padded[1:-1].astype(jnp.float32)
        + tap_table[2] * padded[2:].astype(jnp.float32)
    )
    hidden = (jax.nn.silu(conv_out[:, :half_width]) * conv_out[:, half_width:]).astype(jnp.bfloat16)
    picked = hidden
    ff_out = lax.psum_scatter(
        lax.dot_general(
            picked, down_full, (((1,), (1,)), ((), ())), preferred_element_type=jnp.float32
        ).astype(jnp.bfloat16),
        "tp",
        scatter_dimension=0,
        tiled=True,
    ).astype(jnp.float32)
    return (middle_own.astype(jnp.float32) + ff_out).astype(jnp.bfloat16)


def block_kernel(
    spans,
    shares,
    pieces,
    query,
    key,
    value,
    gate,
    rates,
    gains,
    residual,
    norm_gain,
    gate_taps,
    up_taps,
    out_hbm,
    gate_hbm,
    up_hbm,
    down_hbm,
    result,
    keys,
    values,
    rate_all,
    out_w,
    pair_w,
    down_w,
    att_send,
    att_recv,
    middle_ref,
    norm_send,
    norm_all,
    part_send,
    part_own,
    part_recv,
    hidden_all,
    tp_send,
    tp_recv,
    row_send,
    row_recv,
    local_sem,
    kv_sem,
    att_sem,
    norm_sem,
    fan_sem,
    part_sem,
    hid_sem,
    tp_sem,
    row_sem,
):
    me, lane = lax.axis_index("sp"), lax.axis_index("tp")
    rows, width = query.shape
    heads = width // HEAD
    share = rows // shares
    model = residual.shape[1]
    part_cols = model // spans
    f32, bf16 = jnp.float32, jnp.bfloat16
    sends = []

    def send(src, dst, sems, sp, tp):
        copy = pltpu.make_async_remote_copy(
            src_ref=src,
            dst_ref=dst,
            send_sem=sems.at[0],
            recv_sem=sems.at[1],
            device_id={"sp": sp, "tp": tp},
            device_id_type=pl.DeviceIdType.MESH,
        )
        copy.start()
        sends.append(copy)
        return copy

    def span_at(step):
        return lax.rem(me + step, spans)

    def share_at(step):
        return lax.rem(lane + step, shares)

    def span_rows(index):
        return pl.ds(pl.multiple_of(index * rows, rows), rows)

    loads = [
        pltpu.make_async_copy(src, dst, local_sem.at[i])
        for i, (src, dst) in enumerate(
            (
                (key, keys.at[span_rows(me)]),
                (value, values.at[span_rows(me)]),
                (rates, rate_all.at[me]),
                (out_hbm, out_w),
                (gate_hbm, pair_w.at[0]),
                (up_hbm, pair_w.at[1]),
                (down_hbm, down_w),
            )
        )
    ]
    for load in loads:
        load.start()
    barrier = pltpu.get_barrier_semaphore()
    for a in range(spans):
        for b in range(shares):
            if a or b:
                pl.semaphore_signal(
                    barrier,
                    inc=1,
                    device_id={"sp": span_at(a), "tp": share_at(b)},
                    device_id_type=pl.DeviceIdType.MESH,
                )
    pl.semaphore_wait(barrier, spans * shares - 1)

    arrivals = []
    for d in range(1, spans):
        to = span_at(d)
        arrivals += [
            send(rates, rate_all.at[me], kv_sem.at[d, 0], to, lane),
            send(key, keys.at[span_rows(me)], kv_sem.at[d, 1], to, lane),
            send(value, values.at[span_rows(me)], kv_sem.at[d, 2], to, lane),
        ]
    for load in loads[:3]:
        load.wait()
    for copy in arrivals:
        copy.wait_recv()

    low = lax.broadcasted_iota(jnp.int32, (rows, rows), 0)
    high = lax.broadcasted_iota(jnp.int32, (rows, rows), 1)
    upto = (low <= high).astype(f32)
    since = (low >= high).astype(f32)
    lines = rates.shape[0]
    offset = jnp.zeros((lines, 1), f32)
    offset_own = jnp.zeros((lines, 1), f32)
    cumuls = []
    for j in range(spans):
        offset_own = jnp.where(j == me, offset, offset_own)
        inside = jnp.dot(rate_all[j], upto, precision=FULL_PRECISION, preferred_element_type=f32)
        cumuls.append(inside + offset)
        offset = offset + inside[:, rows - 1 :]
    cumul = jnp.concatenate(cumuls, axis=1)
    every_rate = jnp.concatenate([rate_all[j] for j in range(spans)], axis=1)
    own_rate = rates[...]
    own_cumul = lax.dot_general(
        since,
        own_rate,
        (((1,), (1,)), ((), ())),
        precision=FULL_PRECISION,
        preferred_element_type=f32,
    )
    own_before = lax.dot_general(
        (low > high).astype(f32),
        own_rate,
        (((1,), (1,)), ((), ())),
        precision=FULL_PRECISION,
        preferred_element_type=f32,
    )
    total = spans * rows
    mine_at = lax.broadcasted_iota(jnp.int32, (rows, total), 0) + me * rows
    other_at = lax.broadcasted_iota(jnp.int32, (rows, total), 1)
    mixed = []
    for head in range(heads):
        cols = slice(head * HEAD, (head + 1) * HEAD)
        scores = lax.dot_general(
            query[:, cols],
            keys[:, cols],
            (((1,), (1,)), ((), ())),
            preferred_element_type=f32,
        ) * (HEAD ** (-0.5))
        back = heads + head
        ahead_gap = (own_cumul[:, head : head + 1] + offset_own[head : head + 1]) - cumul[
            head : head + 1
        ]
        behind_gap = (cumul[back : back + 1] - every_rate[back : back + 1]) - (
            own_before[:, back : back + 1] + offset_own[back : back + 1]
        )
        sides = []
        for gap, keep, row in (
            (ahead_gap, mine_at >= other_at, 0),
            (behind_gap, mine_at <= other_at, 1),
        ):
            weighted = jnp.where(keep, jnp.exp(jnp.minimum(gap, 0.0)), 0.0) * scores
            top = weighted.astype(bf16)
            rest = (weighted - top.astype(f32)).astype(bf16)
            held = values[:, cols]
            out = jnp.dot(top, held, preferred_element_type=f32) + jnp.dot(
                rest, held, preferred_element_type=f32
            )
            centre = out - jnp.mean(out, axis=1, keepdims=True)
            spread = jnp.mean(centre * centre, axis=1, keepdims=True)
            sides.append(centre * lax.rsqrt(spread + GROUP_EPS) * gains[row : row + 1, cols])
        level = gate[:, cols].astype(f32)
        mixed.append(((level / (1.0 + jnp.exp(-level))) * (sides[0] + sides[1])).astype(bf16))
    mixed = jnp.concatenate(mixed, axis=1)

    loads[3].wait()
    step_cols = math.gcd(model, 512)
    for at in range(0, model, step_cols):
        att_send[:, at : at + step_cols] = jnp.dot(
            mixed, out_w[:, at : at + step_cols], preferred_element_type=f32
        ).astype(bf16)

    def share_rows(index):
        return pl.ds(pl.multiple_of(index * share, share), share)

    arrivals = [
        send(
            att_send.at[share_rows(share_at(d))],
            att_recv.at[d],
            att_sem.at[d],
            me,
            share_at(d),
        )
        for d in range(1, shares)
    ]
    attended = att_send[share_rows(lane), :].astype(f32)
    for d, copy in enumerate(arrivals, 1):
        copy.wait_recv()
        attended = attended + att_recv[d].astype(f32)
    middle = (residual[share_rows(lane), :].astype(f32) + attended).astype(bf16)
    middle_ref[...] = middle
    middle = middle.astype(f32)
    factor = lax.rsqrt(jnp.mean(middle * middle, axis=1, keepdims=True) + NORM_EPS)
    normed = (middle * factor * norm_gain[...].astype(f32)).astype(bf16)
    for j in range(spans):
        norm_send[j] = normed[:, j * part_cols : (j + 1) * part_cols]

    def token_rows(span, tp):
        return pl.ds(pl.multiple_of(span * rows + tp * share, share), share)

    arrivals = [
        send(
            norm_send.at[span_at(d)],
            norm_all.at[token_rows(me, lane)],
            norm_sem.at[d],
            span_at(d),
            lane,
        )
        for d in range(1, spans)
    ]
    norm_all[token_rows(me, lane), :] = norm_send[me]
    fans = {}
    for d in (0, *range(1, spans)):
        source = lax.rem(me + spans - d, spans)
        if d:
            arrivals[d - 1].wait_recv()
        block = norm_send.at[me] if d == 0 else norm_all.at[token_rows(source, lane)]
        for b in range(1, shares):
            fans[d, b] = send(
                block, norm_all.at[token_rows(source, lane)], fan_sem.at[d, b], me, share_at(b)
            )
    for copy in fans.values():
        copy.wait_recv()

    loads[4].wait()
    loads[5].wait()
    last = spans - 1
    half = spans * rows // 2
    reach = half + EDGE
    size = pieces[0][1]
    origins, owners = (last, 0), (0, last)

    def part_copy(way, c):
        return pltpu.make_async_remote_copy(
            src_ref=part_send.at[way, c],
            dst_ref=part_recv.at[way, c],
            send_sem=part_sem.at[way, c, 0],
            recv_sem=part_sem.at[way, c, 1],
            device_id={"sp": span_at(spans - 1 if way == 0 else 1), "tp": lane},
            device_id_type=pl.DeviceIdType.MESH,
        )

    def hidden_copy(way, c):
        block = hidden_all.at[pl.ds(way * half, half), pl.ds(pieces[c][0], size)]
        return pltpu.make_async_remote_copy(
            src_ref=block,
            dst_ref=block,
            send_sem=hid_sem.at[way, c, 0],
            recv_sem=hid_sem.at[way, c, 1],
            device_id={"sp": span_at(1 if way == 0 else spans - 1), "tp": lane},
            device_id_type=pl.DeviceIdType.MESH,
        )

    def start_part(way, c):
        @pl.when(me == origins[way])
        def _():
            if c >= FLIGHT:
                part_copy(way, c - FLIGHT).wait_send()
            part_copy(way, c).start()

    def start_hidden(way, c):
        @pl.when(me == owners[way])
        def _():
            if c >= FLIGHT:
                hidden_copy(way, c - FLIGHT).wait_send()
            hidden_copy(way, c).start()

    def project(c):
        cols = slice(pieces[c][0], pieces[c][0] + size)
        for way in range(2):
            at = way * (half - EDGE)
            block = norm_all[at : at + reach, :]
            products = [
                jnp.dot(block, pair_w[g, :, cols], preferred_element_type=f32) for g in range(2)
            ]

            @pl.when(me == origins[way])
            def _():
                for g in range(2):
                    part_send[way, c, g] = products[g].astype(bf16)

            start_part(way, c)

            @pl.when(me != origins[way])
            def _():
                for g in range(2):
                    part_own[way, c, g] = products[g]

    for c in range(min(HEADSTART, len(pieces))):
        project(c)

    row_at = lax.broadcasted_iota(jnp.int32, (reach, 1), 0)
    issued = 0
    hops = (last - me, me)
    for turn in range(len(pieces) + SKEW * (last - 1)):
        if turn + HEADSTART < len(pieces):
            project(turn + HEADSTART)
        for way in range(2):
            for hop in range(1, last):
                c = turn - SKEW * (hop - 1)
                if 0 <= c < len(pieces):

                    @pl.when(hops[way] == hop)
                    def _():
                        part_copy(way, c).wait_recv()
                        for g in range(2):
                            part_send[way, c, g] = (
                                part_own[way, c, g] + part_recv[way, c, g].astype(f32)
                            ).astype(bf16)
                        part_copy(way, c).start()

            c = turn - SKEW * (last - 1)
            if c < 0:
                continue
            cols = slice(pieces[c][0], pieces[c][0] + size)

            @pl.when(me == owners[way])
            def _():
                part_copy(way, c).wait_recv()
                convs = []
                for g, taps in enumerate((gate_taps, up_taps)):
                    here = (part_own[way, c, g] + part_recv[way, c, g].astype(f32)).astype(bf16)
                    here = here.astype(f32)
                    earlier, later = pltpu.roll(here, 1, 0), pltpu.roll(here, reach - 1, 0)
                    if way == 0:
                        earlier = jnp.where(row_at == 0, 0.0, earlier)
                    else:
                        later = jnp.where(row_at == reach - 1, 0.0, later)
                    weight = taps[:, cols].astype(f32)
                    convs.append(weight[0:1] * earlier + weight[1:2] * here + weight[2:3] * later)
                hidden = ((convs[0] / (1.0 + jnp.exp(-convs[0]))) * convs[1]).astype(bf16)
                at = way * EDGE
                hidden_all[way * half : (way + 1) * half, cols] = hidden[at : at + half]

        ready = min(max(0, turn - SKEW * (last - 1) + 1), len(pieces))
        if ready < len(pieces):
            ready = min(ready, 2 * max(0, turn + 1 + HEADSTART - len(pieces)))
        while issued < ready:
            for way in range(2):
                start_hidden(way, issued)
            issued += 1

    for turn in range(len(pieces) + SKEW * (last - 1)):
        for way in range(2):
            for hop in range(1, spans):
                c = turn - SKEW * (hop - 1)
                if 0 <= c < len(pieces):

                    @pl.when(last - hops[way] == hop)
                    def _():
                        hidden_copy(way, c).wait_recv()
                        if hop < last:
                            hidden_copy(way, c).start()

    loads[6].wait()
    near_first = list(range(spans))
    fans = {}
    for d in near_first:
        source = lax.rem(me + spans - d, spans)
        tp_send[d] = lax.dot_general(
            hidden_all[span_rows(source), :],
            down_w[...],
            (((1,), (1,)), ((), ())),
            preferred_element_type=f32,
        ).astype(bf16)
        for b in range(1, shares):
            fans[d, b] = send(
                tp_send.at[d, share_rows(share_at(b))],
                tp_recv.at[d, b],
                tp_sem.at[d, b],
                me,
                share_at(b),
            )
    arrivals = []
    for d in near_first:
        source = lax.rem(me + spans - d, spans)
        summed = tp_send[d, share_rows(lane), :].astype(f32)
        for b in range(1, shares):
            fans[d, b].wait_recv()
            summed = summed + tp_recv[d, b].astype(f32)
        row_send[d] = summed.astype(bf16)
        if d:
            arrivals.append(send(row_send.at[d], row_recv.at[me], row_sem.at[d], source, lane))
        else:
            row_recv[me] = row_send[0]
    for copy in arrivals:
        copy.wait_recv()
    for j in range(spans):
        cols = slice(j * part_cols, (j + 1) * part_cols)
        result[:, cols] = (middle_ref[:, cols].astype(f32) + row_recv[j].astype(f32)).astype(bf16)
    for copy in sends:
        copy.wait_send()
    for c in range(len(pieces)):
        for way in range(2):

            middle_span = (me != owners[way]) & (me != origins[way])
            unwaited = c + FLIGHT >= len(pieces)

            @pl.when(middle_span | ((me == origins[way]) & unwaited))
            def _():
                part_copy(way, c).wait_send()

            @pl.when(middle_span | ((me == owners[way]) & unwaited))
            def _():
                hidden_copy(way, c).wait_send()


def fused_block(
    query_rows,
    key_rows,
    value_rows,
    gate_rows,
    log_decay,
    head_gain,
    out_weight,
    residual,
    norm_gain,
    gate_weight,
    up_weight,
    down_weight,
    gate_taps,
    up_taps,
):
    spans, shares = (lax.axis_size("sp"), lax.axis_size("tp"))
    rows, width = query_rows.shape
    model = residual.shape[1]
    units = gate_weight.shape[1]
    part_cols, share = (model // spans, rows // shares)
    total = spans * rows
    lanes = units // 128
    count = max(n for n in range(1, PIECES + 1) if lanes % n == 0)
    size = units // count
    pieces = [(c * size, size) for c in range(count)]
    reach = total // 2 + EDGE
    lines = log_decay.shape[0] * log_decay.shape[1]
    rates = log_decay.reshape(lines, rows)
    f32, bf16 = jnp.float32, jnp.bfloat16
    vmem = pl.BlockSpec(memory_space=pltpu.VMEM)
    far = pl.BlockSpec(memory_space=pl.ANY)
    dma = pltpu.SemaphoreType.DMA
    return pl.pallas_call(
        functools.partial(block_kernel, spans, shares, tuple(pieces)),
        out_shape=jax.ShapeDtypeStruct((share, model), bf16),
        in_specs=[vmem] * 10 + [far] * 4,
        out_specs=vmem,
        scratch_shapes=[
            pltpu.VMEM((total, width), bf16),
            pltpu.VMEM((total, width), bf16),
            pltpu.VMEM((spans, lines, rows), f32),
            pltpu.VMEM(out_weight.shape, bf16),
            pltpu.VMEM((2, *gate_weight.shape), bf16),
            pltpu.VMEM(down_weight.shape, bf16),
            pltpu.VMEM((rows, model), bf16),
            pltpu.VMEM((shares, share, model), bf16),
            pltpu.VMEM((share, model), bf16),
            pltpu.VMEM((spans, share, part_cols), bf16),
            pltpu.VMEM((total, part_cols), bf16),
            pltpu.VMEM((2, count, 2, reach, size), bf16),
            pltpu.VMEM((2, count, 2, reach, size), f32),
            pltpu.VMEM((2, count, 2, reach, size), bf16),
            pltpu.VMEM((total, units), bf16),
            pltpu.VMEM((spans, rows, part_cols), bf16),
            pltpu.VMEM((spans, shares, share, part_cols), bf16),
            pltpu.VMEM((spans, share, part_cols), bf16),
            pltpu.VMEM((spans, share, part_cols), bf16),
            dma((7,)),
            dma((spans, 3, 2)),
            dma((shares, 2)),
            dma((spans, 2)),
            dma((spans, shares, 2)),
            dma((2, count, 2)),
            dma((2, count, 2)),
            dma((spans, shares, 2)),
            dma((spans, 2)),
        ],
        compiler_params=pltpu.CompilerParams(collective_id=0, has_side_effects=True),
    )(
        query_rows,
        key_rows,
        value_rows,
        gate_rows,
        rates,
        head_gain,
        residual,
        norm_gain.reshape(1, model),
        gate_taps,
        up_taps,
        out_weight,
        gate_weight,
        up_weight,
        down_weight,
    )


def either(*args):
    span_tokens = args[0].shape[0] * lax.axis_size("sp")
    model_width = args[7].shape[1]
    if span_tokens < model_width:
        return fused_block(*args)
    return shards(*args)


def solution(mesh):
    in_specs = (
        P(("grp", "sp"), "tp"),
        P(("grp", "sp"), "tp"),
        P(("grp", "sp"), "tp"),
        P(("grp", "sp"), "tp"),
        P(None, "tp", ("grp", "sp")),
        P(None, "tp"),
        P("tp", None),
        P(("grp", "sp"), None),
        P(),
        P("sp", "tp"),
        P("sp", "tp"),
        P("sp", "tp"),
        P(None, "tp"),
        P(None, "tp"),
    )
    out_specs = P(("grp", "sp", "tp"), None)
    return jax.shard_map(either, mesh=mesh, in_specs=in_specs, out_specs=out_specs, check_vma=False)
```

profile of v0, /device:TPU:0, one launch (start us, length us, event | category | flops | bytes accessed | tf_op | source)
XLA Modules:
  0.0 114.6 jit_solution(15502885379068143933)
XLA Ops:
  0.0 1.3 %reshape.7.norm_gain = bf16[1,2048]{1,0:T(2,128)(2,1)} reshape(bf16[2048]{0:T(1024)(128)(2,1)} %param.22) | data formatting | bytes 8192 | tf_op jit(solution)/shard_map/reshape | solution.py:712
  1.3 111.7 %shard_map.136 = bf16[32,2048]{1,0:T(8,128)(2,1)} custom-call(bf16[128,256]{1,0:T(8,128)(2,1)} %query.1, bf16[128,256]{1,0:T(8,128)(2,1)} %key.1, bf16[128,256]{1,0:T(8,128)(2,1)} %value.1, bf16[128,256]{1,0:T(8,128)(2,1)} %gate.1, f32[4,128]{1,0:T(4,128)} %bitcast.1, f32[2,256]{1,0:T(2,128)} %gains.1, bf16[128,2048]{1,0:T(8,128)(2,1)} %residual.1, ...), custom_call_target="tpu_custom_call" | custom-call | tf_op jit(solution)/shard_map/pallas_call | solution.py:668
  113.0 1.6 %copy.16 = bf16[32,2048]{1,0:T(8,128)(2,1)} copy(bf16[32,2048]{1,0:T(8,128)(2,1)} %shard_map.136) | data formatting | bytes 262144
where the time goes:
time: 115 us
  Pallas kernels  112 us (97%)
  local copies, waits for them, and re-layouts  2.86 us (2%)
    pallas_call x1, Pallas kernels, fused_block(): pl.pallas_call(functools.partial(block_kernel, spans, shares, tuple(piece...  112 us

commit v1 on v0

v1 whole, which is shorter than its diff:
```python
import functools
import math

import jax
import jax.numpy as jnp
from jax import lax
from jax.experimental import pallas as pl
from jax.experimental.pallas import tpu as pltpu
from jax.sharding import PartitionSpec as P

HEAD = 128


FULL_PRECISION = lax.Precision.HIGHEST
GROUP_EPS = 1e-05
NORM_EPS = 1e-06


def prefix(value, axis, join, neutral, backward):
    count, mine = (lax.axis_size(axis), lax.axis_index(axis))
    pieces = jax.tree.map(lambda part: lax.all_gather(part, axis), value)
    if backward:
        pieces = jax.tree.map(lambda part: part[::-1], pieces)
        mine = count - 1 - mine
    running = jax.tree.map(
        lambda part, zero: jnp.full_like(part, 0) + jnp.asarray(zero, part.dtype), value, neutral
    )

    def lap(position, running):
        longer = join(running, jax.tree.map(lambda part: part[position], pieces))
        return jax.tree.map(lambda new, old: jnp.where(position < mine, new, old), longer, running)

    return lax.fori_loop(0, count - 1, lap, running)


def padded_2(shard, sides, width):
    for axis, dim in sides:
        size, length = (lax.axis_size(axis), shard.shape[dim])
        up = [(i, (i + 1) % size) for i in range(size - 1)]
        down = [(j, i) for i, j in up]
        last = lax.slice_in_dim(shard, length - width, length, axis=dim)
        initial = lax.slice_in_dim(shard, 0, width, axis=dim)
        before = lax.ppermute(last, axis, up)
        after = lax.ppermute(initial, axis, down)
        shard = jnp.concatenate([before, shard, after], axis=dim)
    return shard


def state_combine(earlier, later):
    return (earlier[0] * later[0], earlier[1] * later[0][:, None, None] + later[1])


def group_norm(values):
    length, head_count, head_width = values.shape
    centre = values - jnp.mean(values, axis=2, keepdims=True)
    spread = jnp.mean(centre * centre, axis=2, keepdims=True)
    return (centre * lax.rsqrt(spread + GROUP_EPS)).reshape(length, head_count * head_width)


def rms_scale(middle, gain):
    values = middle.astype(jnp.float32)
    multiplier = lax.rsqrt(jnp.mean(values * values, axis=1, keepdims=True) + NORM_EPS)
    return (values * multiplier * gain.astype(jnp.float32)).astype(jnp.bfloat16)


def local_retention(query_all, key_all, value_all, log_rates):
    length, head_count, head_width = query_all.shape
    block_len = math.gcd(length, 512)
    block_count = length // block_len
    cumul = jnp.cumsum(log_rates, axis=1).T
    query_block = query_all.reshape(block_count, block_len, head_count, head_width)
    key_block = key_all.reshape(block_count, block_len, head_count, head_width)
    value_block = value_all.reshape(block_count, block_len, head_count, head_width)
    cumul_block = cumul.reshape(block_count, block_len, head_count)
    before = jnp.concatenate(
        [jnp.zeros((1, head_count), jnp.float32), cumul_block[:-1, -1]], axis=0
    )
    local_cumul = cumul_block - before[:, None, :]
    gap_logs = local_cumul[:, :, None, :] - local_cumul[:, None, :, :]
    lower_mask = (jnp.arange(block_len)[:, None] >= jnp.arange(block_len)[None, :])[
        None, :, :, None
    ]
    decay_mask = jnp.where(lower_mask, jnp.exp(jnp.minimum(gap_logs, 0.0)), 0.0)
    scores = (
        jnp.einsum("bthd,bshd->btsh", query_block, key_block, precision=FULL_PRECISION) * decay_mask
    )
    inner_part = jnp.einsum("btsh,bshe->bthe", scores, value_block, precision=FULL_PRECISION)
    to_end = jnp.exp(local_cumul[:, -1:, :] - local_cumul)
    block_states = jnp.einsum(
        "bshd,bshe->bhde", key_block * to_end[..., None], value_block, precision=FULL_PRECISION
    )
    block_decay = jnp.exp(local_cumul[:, -1, :])

    def carry_step(carry_state, inputs):
        return (carry_state * inputs[0][:, None, None] + inputs[1], carry_state)

    zero_state = jnp.zeros((head_count, head_width, head_width), jnp.float32)
    end_state, entering = lax.scan(carry_step, zero_state, (block_decay, block_states))
    carried = jnp.einsum(
        "bthd,bhde->bthe",
        query_block * jnp.exp(local_cumul)[..., None],
        entering,
        precision=FULL_PRECISION,
    )
    output = (inner_part + carried).reshape(length, head_count, head_width)
    return (output, end_state, cumul, jnp.exp(cumul[-1]))


def with_incoming(output, query_all, cumul, incoming):
    return output + jnp.einsum(
        "thd,hde->the", query_all * jnp.exp(cumul)[:, :, None], incoming, precision=FULL_PRECISION
    )


def shards(
    query_rows,
    key_rows,
    value_rows,
    gate_rows,
    log_decay,
    head_gain,
    out_weight,
    residual,
    norm_gain,
    gate_weight,
    up_weight,
    down_weight,
    gate_taps,
    up_taps,
):
    pair_local = jnp.concatenate([gate_weight, up_weight], axis=1)
    row_count = query_rows.shape[0]
    head_count = query_rows.shape[1] // HEAD
    key_scale = HEAD ** (-0.5)
    query_all = query_rows.astype(jnp.float32).reshape(row_count, head_count, HEAD)
    key_all = key_rows.astype(jnp.float32).reshape(row_count, head_count, HEAD) * key_scale
    value_all = value_rows.astype(jnp.float32).reshape(row_count, head_count, HEAD)
    identity = (
        jnp.ones((head_count,), jnp.float32),
        jnp.zeros((head_count, HEAD, HEAD), jnp.float32),
    )
    ahead_local, ahead_state, ahead_cumul, ahead_decay = local_retention(
        query_all, key_all, value_all, log_decay[0]
    )
    query_back = query_all[::-1]
    behind_local, behind_state, behind_cumul, behind_decay = local_retention(
        query_back, key_all[::-1], value_all[::-1], log_decay[1][:, ::-1]
    )
    ahead_in = prefix((ahead_decay, ahead_state), "sp", state_combine, identity, False)[1]
    behind_in = prefix((behind_decay, behind_state), "sp", state_combine, identity, True)[1]
    ahead_out = with_incoming(ahead_local, query_all, ahead_cumul, ahead_in)
    behind_out = with_incoming(behind_local, query_back, behind_cumul, behind_in)[::-1]
    combined = group_norm(ahead_out) * head_gain[0] + group_norm(behind_out) * head_gain[1]
    mixed_heads = (jax.nn.silu(gate_rows.astype(jnp.float32)) * combined).astype(jnp.bfloat16)
    gathered = (
        lax.all_gather(pair_local, "sp", axis=0, tiled=True),
        lax.all_gather(down_weight, "sp", axis=0, tiled=True),
    )
    pair_full, down_full = gathered
    share_rows = row_count // lax.axis_size("tp")
    own_start = lax.axis_index("tp") * share_rows
    picked = mixed_heads
    attended = lax.psum_scatter(
        jnp.dot(picked, out_weight, preferred_element_type=jnp.float32).astype(jnp.bfloat16),
        "tp",
        scatter_dimension=0,
        tiled=True,
    ).astype(jnp.float32)
    residual_own = lax.dynamic_slice_in_dim(residual, own_start, share_rows, 0)
    middle_own = lax.optimization_barrier(
        (residual_own.astype(jnp.float32) + attended).astype(jnp.bfloat16)
    )
    normed = rms_scale(middle_own, norm_gain)
    pre_both = jnp.dot(
        lax.all_gather(normed, "tp", axis=0, tiled=True),
        pair_full,
        preferred_element_type=jnp.float32,
    ).astype(jnp.bfloat16)
    padded = padded_2(pre_both, (("sp", 0),), 1)
    half_width = gate_taps.shape[1]
    tap_table = jnp.concatenate([gate_taps, up_taps], axis=1).astype(jnp.float32)
    conv_out = (
        tap_table[0] * padded[:-2].astype(jnp.float32)
        + tap_table[1] * padded[1:-1].astype(jnp.float32)
        + tap_table[2] * padded[2:].astype(jnp.float32)
    )
    hidden = (jax.nn.silu(conv_out[:, :half_width]) * conv_out[:, half_width:]).astype(jnp.bfloat16)
    picked = hidden
    ff_out = lax.psum_scatter(
        lax.dot_general(
            picked, down_full, (((1,), (1,)), ((), ())), preferred_element_type=jnp.float32
        ).astype(jnp.bfloat16),
        "tp",
        scatter_dimension=0,
        tiled=True,
    ).astype(jnp.float32)
    return (middle_own.astype(jnp.float32) + ff_out).astype(jnp.bfloat16)


def tile_split(lanes, spans):
    least, rest = divmod(lanes, spans)
    return least, rest


def block_kernel(
    spans,
    shares,
    query_hbm,
    key_hbm,
    value_hbm,
    gate_hbm,
    rates_hbm,
    gains,
    residual_hbm,
    norm_gain,
    gate_taps,
    up_taps,
    out_hbm,
    fg_hbm,
    fu_hbm,
    down_hbm,
    result,
    query,
    key,
    value,
    gate,
    rates,
    residual,
    out_w,
    down_w,
    rate_all,
    state_send,
    state_recv,
    wide_a,
    wide_b,
    att_send,
    att_recv,
    middle_ref,
    norm_all,
    hid_all,
    tp_send,
    tp_recv,
    row_send,
    row_recv,
    local_sem,
    own_sem,
    state_sem,
    w_sem,
    relay_sem,
    att_sem,
    norm_sem,
    mate_sem,
    cross_sem,
    diag_sem,
    hid_sem,
    tp_sem,
    row_sem,
):
    side, me, lane = lax.axis_index("grp"), lax.axis_index("sp"), lax.axis_index("tp")
    rows, width = query.shape
    heads = width // HEAD
    share = rows // shares
    model = residual.shape[1]
    part_cols = model // spans
    half = part_cols // 2
    total = spans * rows
    lines = rates.shape[0]
    units = gate_taps.shape[1]
    least, rest = tile_split(units // 128, spans)
    f32, bf16 = jnp.float32, jnp.bfloat16
    mate = lane + 1 - 2 * lax.rem(lane, 2)
    cross = lax.rem(lane + shares // 2, shares)
    odd = lax.rem(lane, 2)
    sends = []

    def remote(src, dst, sems, **place):
        return pltpu.make_async_remote_copy(
            src_ref=src,
            dst_ref=dst,
            send_sem=sems.at[0],
            recv_sem=sems.at[1],
            device_id=place,
            device_id_type=pl.DeviceIdType.MESH,
        )

    def send(src, dst, sems, **place):
        copy = remote(src, dst, sems, **place)
        copy.start()
        sends.append(copy)
        return copy

    def span_at(step):
        return lax.rem(me + step, spans)

    def share_at(step):
        return lax.rem(lane + step, shares)

    def extra(span):
        return jnp.where(odd == 0, span < rest, span >= spans - rest)

    def first_col(span):
        before = jnp.where(
            odd == 0, jnp.minimum(span, rest), jnp.maximum(span - (spans - rest), 0)
        )
        return (span * least + before) * 128

    def cols_of(part, span):
        size = 128 if part else least * 128
        begin = jnp.minimum(first_col(span) + part * least * 128, units - size)
        return pl.ds(pl.multiple_of(begin, 128), size)

    barrier = pltpu.get_barrier_semaphore()
    peers = [{"grp": 1 - side}]
    peers += [{"sp": span_at(d)} for d in range(1, spans)]
    peers += [{"tp": share_at(d)} for d in range(1, shares)]
    for place in peers:
        pl.semaphore_signal(
            barrier, inc=1, device_id=place, device_id_type=pl.DeviceIdType.MESH
        )
    loads = [
        pltpu.make_async_copy(src, dst, local_sem.at[i])
        for i, (src, dst) in enumerate(
            (
                (rates_hbm, rates),
                (key_hbm, key),
                (value_hbm, value),
                (query_hbm, query),
                (gate_hbm, gate),
                (out_hbm, out_w),
                (residual_hbm, residual),
                (down_hbm, down_w),
            )
        )
    ]
    for load in loads:
        load.start()

    wides = (wide_a, wide_b)
    weights = (fg_hbm, fu_hbm)

    def own_copy(part, g):
        return pltpu.make_async_copy(
            weights[g].at[:, cols_of(part, me)],
            wides[part].at[g, pl.ds(pl.multiple_of(me * part_cols, part_cols), part_cols)],
            own_sem.at[part, g],
        )

    def half_rows(span):
        begin = span * part_cols + side * half
        return pl.ds(pl.multiple_of(begin, half), half)

    def weight_copy(part, d, g):
        to = span_at(d)
        return remote(
            weights[g].at[pl.ds(pl.multiple_of(side * half, half), half), cols_of(part, to)],
            wides[part].at[g, half_rows(me)],
            w_sem.at[part, d, g],
            sp=to,
        )

    def relay_copy(part, d, g):
        block = wides[part].at[g, half_rows(lax.rem(me + spans - d, spans))]
        return remote(block, block, relay_sem.at[part, d, g], grp=1 - side)

    def when_extra(part, span, step):
        if part:
            pl.when(extra(span))(step)
        else:
            step()

    def start_weights(part, d):
        def step():
            for g in range(2):
                weight_copy(part, d, g).start()

        when_extra(part, span_at(d), step)

    def relay_weights(part, d):
        def step():
            for g in range(2):
                weight_copy(part, d, g).wait_recv()
                relay_copy(part, d, g).start()

        when_extra(part, me, step)

    def own_weights(part, begin):
        def step():
            for g in range(2):
                if begin:
                    own_copy(part, g).start()
                else:
                    own_copy(part, g).wait()

        when_extra(part, me, step)

    for part in range(2):
        own_weights(part, True)

    with jax.named_scope("states"):
        loads[0].wait()
        low = lax.broadcasted_iota(jnp.int32, (rows, rows), 0)
        high = lax.broadcasted_iota(jnp.int32, (rows, rows), 1)
        rate = rates[...]

        def tall(table):
            return lax.dot_general(
                table.astype(f32),
                rate,
                (((1,), (1,)), ((), ())),
                precision=FULL_PRECISION,
                preferred_element_type=f32,
            )

        until = tall(low >= high)
        single = tall(low == high)
        after = tall(low < high)
        flat = jnp.dot(
            rate, (low <= high).astype(f32), precision=FULL_PRECISION, preferred_element_type=f32
        )
        loads[1].wait()
        loads[2].wait()

        def split(x):
            top = x.astype(bf16)
            return top, (x - top.astype(f32)).astype(bf16)

        for head in range(heads):
            cols = slice(head * HEAD, (head + 1) * HEAD)
            held = value[:, cols]
            for way in range(2):
                line = way * heads + head
                if way == 0:
                    weight = after[:, line : line + 1]
                else:
                    weight = until[:, line : line + 1] - single[:, line : line + 1]
                lifted = key[:, cols].astype(f32) * jnp.exp(jnp.minimum(weight, 0.0))
                state = jnp.zeros((HEAD, HEAD), f32)
                for piece in split(lifted):
                    state += lax.dot_general(
                        piece, held, (((0,), (0,)), ((), ())), preferred_element_type=f32
                    )
                state = state - jnp.mean(state, axis=1, keepdims=True)
                state_send[way, head] = state.astype(bf16)

    with jax.named_scope("barrier"):
        pl.semaphore_wait(barrier, len(peers))
    arrivals = []
    for d in range(1, spans):
        to = span_at(d)
        way = jnp.where(to > me, 0, 1)
        arrivals.append(send(rates, rate_all.at[me], state_sem.at[d, 0], sp=to))
        arrivals.append(
            send(state_send.at[way], state_recv.at[me], state_sem.at[d, 1], sp=to)
        )
    start_weights(0, 1)
    start_weights(0, 2)

    with jax.named_scope("inner"):
        loads[3].wait()
        inner = []
        for head in range(heads):
            cols = slice(head * HEAD, (head + 1) * HEAD)
            back = heads + head
            scores = lax.dot_general(
                query[:, cols],
                key[:, cols],
                (((1,), (1,)), ((), ())),
                preferred_element_type=f32,
            ) * (HEAD ** (-0.5))
            ahead_gap = until[:, head : head + 1] - flat[head : head + 1]
            behind_gap = (flat[back : back + 1] - rate[back : back + 1]) - (
                until[:, back : back + 1] - single[:, back : back + 1]
            )
            for gap, keep in ((ahead_gap, low >= high), (behind_gap, low <= high)):
                weighted = jnp.where(keep, jnp.exp(jnp.minimum(gap, 0.0)), 0.0) * scores
                out = jnp.zeros((rows, HEAD), f32)
                for piece in split(weighted):
                    out += jnp.dot(piece, value[:, cols], preferred_element_type=f32)
                inner.append(out)

    with jax.named_scope("state_wait"):
        for copy in arrivals:
            copy.wait_recv()
        loads[4].wait()
    with jax.named_scope("outer"):
        sums = [jnp.sum(rate_all[j], axis=1, keepdims=True) for j in range(spans)]
        mixed = []
        gaps = []
        for j in range(spans):
            ahead_far = jnp.zeros((lines, 1), f32)
            behind_far = jnp.zeros((lines, 1), f32)
            for i in range(spans):
                if i > j:
                    ahead_far += jnp.where(i < me, sums[i], 0.0)
                if i < j:
                    behind_far += jnp.where(i > me, sums[i], 0.0)
            gaps.append((ahead_far, behind_far))
        for head in range(heads):
            cols = slice(head * HEAD, (head + 1) * HEAD)
            back = heads + head
            ahead, behind = inner[2 * head], inner[2 * head + 1]
            for j in range(spans):
                product = jnp.dot(
                    query[:, cols], state_recv[j, head], preferred_element_type=f32
                ) * (HEAD ** (-0.5))
                near = until[:, head : head + 1] + gaps[j][0][head : head + 1]
                far = (
                    after[:, back : back + 1]
                    + single[:, back : back + 1]
                    + gaps[j][1][back : back + 1]
                )
                ahead += jnp.where(j < me, jnp.exp(jnp.minimum(near, 0.0)) * product, 0.0)
                behind += jnp.where(j > me, jnp.exp(jnp.minimum(far, 0.0)) * product, 0.0)
            sides = []
            for row, out in enumerate((ahead, behind)):
                centre = out - jnp.mean(out, axis=1, keepdims=True)
                spread = jnp.mean(centre * centre, axis=1, keepdims=True)
                sides.append(centre * lax.rsqrt(spread + GROUP_EPS) * gains[row : row + 1, cols])
            level = gate[:, cols].astype(f32)
            mixed.append(((level / (1.0 + jnp.exp(-level))) * (sides[0] + sides[1])).astype(bf16))
        mixed = jnp.concatenate(mixed, axis=1)

    def share_rows(index):
        return pl.ds(pl.multiple_of(index * share, share), share)

    with jax.named_scope("attend"):
        loads[5].wait()
        step_cols = math.gcd(model, 512)
        for at in range(0, model, step_cols):
            att_send[:, at : at + step_cols] = jnp.dot(
                mixed, out_w[:, at : at + step_cols], preferred_element_type=f32
            ).astype(bf16)
        arrivals = [
            send(
                att_send.at[share_rows(share_at(d))],
                att_recv.at[d],
                att_sem.at[d],
                tp=share_at(d),
            )
            for d in range(1, shares)
        ]
    with jax.named_scope("relay1"):
        relay_weights(0, 1)
    with jax.named_scope("attended_wait"):
        loads[6].wait()
        for copy in arrivals:
            copy.wait_recv()

    def token_rows(span, tp):
        return pl.ds(pl.multiple_of(span * rows + tp * share, share), share)

    with jax.named_scope("normed"):
        attended = att_send[share_rows(lane), :].astype(f32)
        for d in range(1, shares):
            attended = attended + att_recv[d].astype(f32)
        middle = (residual[share_rows(lane), :].astype(f32) + attended).astype(bf16)
        middle_ref[...] = middle
        middle = middle.astype(f32)
        factor = lax.rsqrt(jnp.mean(middle * middle, axis=1, keepdims=True) + NORM_EPS)
        normed = (middle * factor * norm_gain[...].astype(f32)).astype(bf16)
        norm_all[token_rows(me, lane), :] = normed

    steps = (1, -1)

    def origin(way, hop):
        return me - steps[way] * hop

    def inside(span):
        return (span >= 0) & (span < spans)

    def clamp(span):
        return jnp.clip(span, 0, spans - 1)

    def passes(way, hop):
        return inside(origin(way, hop)) & inside(me + steps[way])

    def norm_copy(way, hop):
        block = norm_all.at[token_rows(clamp(origin(way, hop)), lane)]
        return remote(
            block, block, norm_sem.at[way, hop], sp=clamp(me + steps[way])
        )

    def mate_copy(span):
        block = norm_all.at[token_rows(span, lane)]
        return remote(block, block, mate_sem.at[span], tp=mate)

    def cross_copy(span):
        block = norm_all.at[token_rows(span, lane)]
        return remote(block, block, cross_sem.at[span], tp=cross)

    def diag_copy(span):
        block = norm_all.at[token_rows(span, cross)]
        return remote(block, block, diag_sem.at[span], tp=mate)

    def spread_block(way, hop):
        if hop + 1 >= spans:
            return

        @pl.when(passes(way, hop))
        def _():
            norm_copy(way, hop).start()

    def norm_hop(hop):
        for way in range(2):

            @pl.when(inside(origin(way, hop)))
            def _():
                norm_copy(way, hop - 1).wait_recv()
                spread_block(way, hop)
                cross_copy(clamp(origin(way, hop))).start()
                mate_copy(clamp(origin(way, hop))).start()

    def cross_hop(hop):
        for way in range(2 if hop else 1):

            @pl.when(inside(origin(way, hop)))
            def _():
                cross_copy(clamp(origin(way, hop))).wait_recv()
                diag_copy(clamp(origin(way, hop))).start()

    with jax.named_scope("norm0"):
        for way in range(2):
            spread_block(way, 0)
        cross_copy(me).start()
        mate_copy(me).start()
        start_weights(0, 3)
    with jax.named_scope("relay2"):
        relay_weights(0, 2)
    for hop in range(1, spans):
        with jax.named_scope("norm_hop"):
            norm_hop(hop)
            start_weights(1, hop)
            cross_hop(hop - 1)
    with jax.named_scope("norm_last"):
        cross_hop(spans - 1)
        for span in range(spans):
            mate_copy(span).wait_recv()
            diag_copy(span).wait_recv()
    with jax.named_scope("relay3"):
        relay_weights(0, 3)
        own_weights(0, False)
        for d in range(1, spans):
            for g in range(2):
                relay_copy(0, d, g).wait_recv()

    row_at = lax.broadcasted_iota(jnp.int32, (total, 1), 0)

    def compute_hidden(part):
        cols = cols_of(part, me)
        convs = []
        for g, taps in enumerate((gate_taps, up_taps)):
            here = jnp.dot(norm_all[...], wides[part][g], preferred_element_type=f32)
            here = here.astype(bf16).astype(f32)
            earlier, later = pltpu.roll(here, 1, 0), pltpu.roll(here, total - 1, 0)
            earlier = jnp.where(row_at == 0, 0.0, earlier)
            later = jnp.where(row_at == total - 1, 0.0, later)
            weight = taps[:, cols].astype(f32)
            convs.append(weight[0:1] * earlier + weight[1:2] * here + weight[2:3] * later)
        hidden = ((convs[0] / (1.0 + jnp.exp(-convs[0]))) * convs[1]).astype(bf16)
        hid_all[:, cols] = hidden

    def hidden_copy(part, way, hop, b):
        block = hid_all.at[pl.ds(b * rows, rows), cols_of(part, clamp(origin(way, hop)))]
        return remote(
            block, block, hid_sem.at[part, way, hop, b], sp=clamp(me + steps[way])
        )

    def has(part, span):
        return inside(span) & extra(clamp(span)) if part else inside(span)

    def hidden_start(part, way, hop, b):
        if hop + 1 >= spans:
            return

        @pl.when(passes(way, hop) & has(part, origin(way, hop)))
        def _():
            hidden_copy(part, way, hop, b).start()

    def hidden_pass(part, hop, b):
        for way in range(2):

            @pl.when(has(part, origin(way, hop)))
            def _():
                hidden_copy(part, way, hop - 1, b).wait_recv()

            hidden_start(part, way, hop, b)

    with jax.named_scope("hidden_a"):
        compute_hidden(0)
        for b in range(spans):
            for way in range(2):
                hidden_start(0, way, 0, b)
    with jax.named_scope("relay4"):
        for d in range(1, spans):
            relay_weights(1, d)
    with jax.named_scope("relay5"):

        @pl.when(extra(me))
        def _():
            for d in range(1, spans):
                for g in range(2):
                    relay_copy(1, d, g).wait_recv()

        own_weights(1, False)
    with jax.named_scope("hidden_b"):

        @pl.when(extra(me))
        def _():
            compute_hidden(1)

        for b in range(spans):
            for way in range(2):
                hidden_start(1, way, 0, b)
    with jax.named_scope("pass_a"):
        for hop in range(1, spans):
            for b in range(spans):
                hidden_pass(0, hop, b)
    loads[7].wait()
    fans = {}
    for b in range(spans):
        with jax.named_scope("pass_b"):
            for hop in range(1, spans):
                hidden_pass(1, hop, b)
        with jax.named_scope("down"):
            tp_send[b] = lax.dot_general(
                hid_all[b * rows : (b + 1) * rows, :],
                down_w[...],
                (((1,), (1,)), ((), ())),
                preferred_element_type=f32,
            ).astype(bf16)
            for d in range(1, shares):
                fans[b, d] = send(
                    tp_send.at[b, share_rows(share_at(d))],
                    tp_recv.at[b, d],
                    tp_sem.at[b, d],
                    tp=share_at(d),
                )

    def row_out(b):
        d = lax.rem(b - me + spans, spans)
        return remote(row_send.at[b], row_recv.at[me], row_sem.at[d], sp=b)

    for b in range(spans):
        with jax.named_scope("rows"):
            summed = tp_send[b, share_rows(lane), :].astype(f32)
            for d in range(1, shares):
                fans[b, d].wait_recv()
                summed = summed + tp_recv[b, d].astype(f32)
            row_send[b] = summed.astype(bf16)

            @pl.when(b != me)
            def _():
                row_out(b).start()

            @pl.when(b == me)
            def _():
                row_recv[me] = row_send[b]

    with jax.named_scope("final"):
        for d in range(1, spans):
            row_out(span_at(d)).wait_recv()
        for j in range(spans):
            cols = slice(j * part_cols, (j + 1) * part_cols)
            result[:, cols] = (
                middle_ref[:, cols].astype(f32) + row_recv[j].astype(f32)
            ).astype(bf16)
    with jax.named_scope("drain"):
        for copy in sends:
            copy.wait_send()
        for part in range(2):
            for d in range(1, spans):

                def sent():
                    for g in range(2):
                        weight_copy(part, d, g).wait_send()

                def relayed():
                    for g in range(2):
                        relay_copy(part, d, g).wait_send()

                when_extra(part, span_at(d), sent)
                when_extra(part, me, relayed)
        for span in range(spans):
            cross_copy(span).wait_send()
            mate_copy(span).wait_send()
            diag_copy(span).wait_send()

            @pl.when(span != me)
            def _():
                row_out(span).wait_send()

        for way in range(2):
            for hop in range(spans - 1):

                @pl.when(passes(way, hop))
                def _():
                    norm_copy(way, hop).wait_send()

                for part in range(2):

                    @pl.when(passes(way, hop) & has(part, origin(way, hop)))
                    def _():
                        for b in range(spans):
                            hidden_copy(part, way, hop, b).wait_send()


def fused_block(
    query_rows,
    key_rows,
    value_rows,
    gate_rows,
    log_decay,
    head_gain,
    out_weight,
    residual,
    norm_gain,
    gate_weight,
    up_weight,
    down_weight,
    gate_taps,
    up_taps,
):
    spans, shares = (lax.axis_size("sp"), lax.axis_size("tp"))
    rows, width = query_rows.shape
    model = residual.shape[1]
    units = gate_weight.shape[1]
    part_cols, share = (model // spans, rows // shares)
    total = spans * rows
    least, rest = tile_split(units // 128, spans)
    lines = log_decay.shape[0] * log_decay.shape[1]
    heads = width // HEAD
    rates = log_decay.reshape(lines, rows)
    f32, bf16 = jnp.float32, jnp.bfloat16
    far = pl.BlockSpec(memory_space=pl.ANY)
    near = pl.BlockSpec(memory_space=pltpu.VMEM)
    dma = pltpu.SemaphoreType.DMA
    vmem = pltpu.VMEM
    return pl.pallas_call(
        functools.partial(block_kernel, spans, shares),
        out_shape=jax.ShapeDtypeStruct((share, model), bf16),
        in_specs=[far] * 5 + [near, far] + [near] * 3 + [far] * 4,
        out_specs=pl.BlockSpec(memory_space=pltpu.VMEM),
        scratch_shapes=[
            vmem((rows, width), bf16),
            vmem((rows, width), bf16),
            vmem((rows, width), bf16),
            vmem((rows, width), bf16),
            vmem((lines, rows), f32),
            vmem((rows, model), bf16),
            vmem(out_weight.shape, bf16),
            vmem(down_weight.shape, bf16),
            vmem((spans, lines, rows), f32),
            vmem((2, heads, HEAD, HEAD), bf16),
            vmem((spans, heads, HEAD, HEAD), bf16),
            vmem((2, model, least * 128), bf16),
            vmem((2, model, 128), bf16),
            vmem((rows, model), bf16),
            vmem((shares, share, model), bf16),
            vmem((share, model), bf16),
            vmem((total, model), bf16),
            vmem((total, units), bf16),
            vmem((spans, rows, part_cols), bf16),
            vmem((spans, shares, share, part_cols), bf16),
            vmem((spans, share, part_cols), bf16),
            vmem((spans, share, part_cols), bf16),
            dma((8,)),
            dma((2, 2)),
            dma((spans, 2, 2)),
            dma((2, spans, 2, 2)),
            dma((2, spans, 2, 2)),
            dma((shares, 2)),
            dma((2, spans, 2)),
            dma((spans, 2)),
            dma((spans, 2)),
            dma((spans, 2)),
            dma((2, 2, spans, spans, 2)),
            dma((spans, shares, 2)),
            dma((spans, 2)),
        ],
        compiler_params=pltpu.CompilerParams(collective_id=0, has_side_effects=True),
    )(
        query_rows,
        key_rows,
        value_rows,
        gate_rows,
        rates,
        head_gain,
        residual,
        norm_gain.reshape(1, model),
        gate_taps,
        up_taps,
        out_weight,
        gate_weight,
        up_weight,
        down_weight,
    )


def either(*args):
    spans, shares, twins = (lax.axis_size(name) for name in ("sp", "tp", "grp"))
    span_tokens = args[0].shape[0] * spans
    model_width = args[7].shape[1]
    lanes = args[9].shape[1] // 128
    if span_tokens < model_width and twins == 2 and shares == 4 and lanes >= spans:
        return fused_block(*args)
    return shards(*args)


def solution(mesh):
    in_specs = (
        P(("grp", "sp"), "tp"),
        P(("grp", "sp"), "tp"),
        P(("grp", "sp"), "tp"),
        P(("grp", "sp"), "tp"),
        P(None, "tp", ("grp", "sp")),
        P(None, "tp"),
        P("tp", None),
        P(("grp", "sp"), None),
        P(),
        P("sp", "tp"),
        P("sp", "tp"),
        P("sp", "tp"),
        P(None, "tp"),
        P(None, "tp"),
    )
    out_specs = P(("grp", "sp", "tp"), None)
    return jax.shard_map(either, mesh=mesh, in_specs=in_specs, out_specs=out_specs, check_vma=False)
```

time: 115 us -> 103 us (0.90)
  Pallas kernels: 112 us -> 99.6 us
    pallas_call x1, Pallas kernels: 112 us -> 99.6 us  [fused_block(): pl.pallas_call(functools.partial(block_kernel, spans, shares), out_shape=...]
where the time goes in v1:
time: 103 us; the launch traced here: 102 us
  Pallas kernels  99.6 us (97%)
  local copies, waits for them, and re-layouts  2.86 us (3%)
    pallas_call x1, Pallas kernels, fused_block(): pl.pallas_call(functools.partial(block_kernel, spans, shares), out_shape=...  99.6 us

profile of v1, /device:TPU:0, one launch (start us, length us, event | category | flops | bytes accessed | tf_op | source)
XLA Modules:
  0.0 102.5 jit_solution(17492469251370437229)
XLA Ops:
  0.0 1.3 %reshape.7.norm_gain = bf16[1,2048]{1,0:T(2,128)(2,1)} reshape(bf16[2048]{0:T(1024)(128)(2,1)} %param.22) | data formatting | bytes 8192 | tf_op jit(solution)/shard_map/reshape | solution.py:889
  1.3 99.6 %shard_map.136 = bf16[32,2048]{1,0:T(8,128)(2,1)} custom-call(bf16[128,256]{1,0:T(8,128)(2,1)} %query_hbm.1, bf16[128,256]{1,0:T(8,128)(2,1)} %key_hbm.1, bf16[128,256]{1,0:T(8,128)(2,1)} %value_hbm.1, bf16[128,256]{1,0:T(8,128)(2,1)} %gate_hbm.1, f32[4,128]{1,0:T(4,128)} %bitcast.1, f32[2,256]{1,0:T(2,128)} %gains.1, bf16[128,2048]{1,0:T(8,128)(2,1)} %residual_hbm.1, ...), custom_call_target="tpu_custom_call" | custom-call | tf_op jit(solution)/shard_map/pallas_call | solution.py:838
  100.9 1.6 %copy.16 = bf16[32,2048]{1,0:T(8,128)(2,1)} copy(bf16[32,2048]{1,0:T(8,128)(2,1)} %shard_map.136) | data formatting | bytes 262144

commit v2 on v1

--- a/solution.py
+++ b/solution.py
@@ -231,8 +231,7 @@
     rate_all,
     state_send,
     state_recv,
-    wide_a,
-    wide_b,
+    wide,
     att_send,
     att_recv,
     middle_ref,
@@ -267,6 +266,7 @@
     lines = rates.shape[0]
     units = gate_taps.shape[1]
     least, rest = tile_split(units // 128, spans)
+    parts = least + (rest > 0)
     f32, bf16 = jnp.float32, jnp.bfloat16
     mate = lane + 1 - 2 * lax.rem(lane, 2)
     cross = lax.rem(lane + shares // 2, shares)
@@ -305,9 +305,8 @@
         return (span * least + before) * 128
 
     def cols_of(part, span):
-        size = 128 if part else least * 128
-        begin = jnp.minimum(first_col(span) + part * least * 128, units - size)
-        return pl.ds(pl.multiple_of(begin, 128), size)
+        begin = jnp.minimum(first_col(span) + part * 128, units - 128)
+        return pl.ds(pl.multiple_of(begin, 128), 128)
 
     barrier = pltpu.get_barrier_semaphore()
     peers = [{"grp": 1 - side}]
@@ -335,15 +334,21 @@
     for load in loads:
         load.start()
 
-    wides = (wide_a, wide_b)
     weights = (fg_hbm, fu_hbm)
+
+    def lanes(g):
+        return slice(g * 128, (g + 1) * 128)
 
     def own_copy(part, g):
         return pltpu.make_async_copy(
             weights[g].at[:, cols_of(part, me)],
-            wides[part].at[g, pl.ds(pl.multiple_of(me * part_cols, part_cols), part_cols)],
-            own_sem.at[part, g],
+            wide.at[part, pl.ds(pl.multiple_of(me * part_cols, part_cols), part_cols), lanes(g)],
+            own_sem.at[part],
         )
+
+    def own_wait(part):
+        block = wide.at[part, pl.ds(pl.multiple_of(me * part_cols, part_cols), part_cols)]
+        return pltpu.make_async_copy(block, block, own_sem.at[part])
 
     def half_rows(span):
         begin = span * part_cols + side * half
@@ -353,17 +358,21 @@
         to = span_at(d)
         return remote(
             weights[g].at[pl.ds(pl.multiple_of(side * half, half), half), cols_of(part, to)],
-            wides[part].at[g, half_rows(me)],
-            w_sem.at[part, d, g],
+            wide.at[part, half_rows(me), lanes(g)],
+            w_sem.at[part, d - 1],
             sp=to,
         )
 
-    def relay_copy(part, d, g):
-        block = wides[part].at[g, half_rows(lax.rem(me + spans - d, spans))]
-        return remote(block, block, relay_sem.at[part, d, g], grp=1 - side)
+    def relay_copy(part, d):
+        block = wide.at[part, half_rows(lax.rem(me + spans - d, spans))]
+        return remote(block, block, relay_sem.at[part, d - 1], grp=1 - side)
+
+    def weight_wait(part, d):
+        block = wide.at[part, half_rows(lax.rem(me + spans - d, spans))]
+        return remote(block, block, w_sem.at[part, d - 1], sp=span_at(d))
 
     def when_extra(part, span, step):
-        if part:
+        if part == least:
             pl.when(extra(span))(step)
         else:
             step()
@@ -377,24 +386,20 @@
 
     def relay_weights(part, d):
         def step():
-            for g in range(2):
-                weight_copy(part, d, g).wait_recv()
-                relay_copy(part, d, g).start()
+            weight_wait(part, d).wait_recv()
+            relay_copy(part, d).start()
 
         when_extra(part, me, step)
 
-    def own_weights(part, begin):
+    def own_weights(part):
         def step():
             for g in range(2):
-                if begin:
-                    own_copy(part, g).start()
-                else:
-                    own_copy(part, g).wait()
+                own_copy(part, g).start()
 
         when_extra(part, me, step)
 
-    for part in range(2):
-        own_weights(part, True)
+    for part in range(parts):
+        own_weights(part)
 
     with jax.named_scope("states"):
         loads[0].wait()
@@ -448,13 +453,10 @@
     for d in range(1, spans):
         to = span_at(d)
         way = jnp.where(to > me, 0, 1)
-        arrivals.append(send(rates, rate_all.at[me], state_sem.at[d, 0], sp=to))
+        arrivals.append(send(rates, rate_all.at[me], state_sem.at[d - 1, 0], sp=to))
         arrivals.append(
-            send(state_send.at[way], state_recv.at[me], state_sem.at[d, 1], sp=to)
+            send(state_send.at[way], state_recv.at[me], state_sem.at[d - 1, 1], sp=to)
         )
-    start_weights(0, 1)
-    start_weights(0, 2)
-
     with jax.named_scope("inner"):
         loads[3].wait()
         inner = []
@@ -482,6 +484,8 @@
         for copy in arrivals:
             copy.wait_recv()
         loads[4].wait()
+        start_weights(0, 1)
+        start_weights(0, 2)
     with jax.named_scope("outer"):
         sums = [jnp.sum(rate_all[j], axis=1, keepdims=True) for j in range(spans)]
         mixed = []
@@ -534,13 +538,11 @@
             send(
                 att_send.at[share_rows(share_at(d))],
                 att_recv.at[d],
-                att_sem.at[d],
+                att_sem.at[d - 1],
                 tp=share_at(d),
             )
             for d in range(1, shares)
         ]
-    with jax.named_scope("relay1"):
-        relay_weights(0, 1)
     with jax.named_scope("attended_wait"):
         loads[6].wait()
         for copy in arrivals:
@@ -557,8 +559,11 @@
         middle_ref[...] = middle
         middle = middle.astype(f32)
         factor = lax.rsqrt(jnp.mean(middle * middle, axis=1, keepdims=True) + NORM_EPS)
-        normed = (middle * factor * norm_gain[...].astype(f32)).astype(bf16)
-        norm_all[token_rows(me, lane), :] = normed
+        for at in range(0, model, 128):
+            gain = norm_gain[at // 128 : at // 128 + 1, :].astype(f32)
+            norm_all[token_rows(me, lane), at : at + 128] = (
+                middle[:, at : at + 128] * factor * gain
+            ).astype(bf16)
 
     steps = (1, -1)
 
@@ -574,11 +579,16 @@
     def passes(way, hop):
         return inside(origin(way, hop)) & inside(me + steps[way])
 
-    def norm_copy(way, hop):
-        block = norm_all.at[token_rows(clamp(origin(way, hop)), lane)]
-        return remote(
-            block, block, norm_sem.at[way, hop], sp=clamp(me + steps[way])
-        )
+    slabs = 2
+    slab = share // slabs
+
+    def slab_rows(span, tp, c):
+        begin = span * rows + tp * share + c * slab
+        return pl.ds(pl.multiple_of(begin, slab), slab)
+
+    def norm_copy(way, hop, c):
+        block = norm_all.at[slab_rows(clamp(origin(way, hop)), lane, c)]
+        return remote(block, block, norm_sem.at[way, hop, c], sp=clamp(me + steps[way]))
 
     def mate_copy(span):
         block = norm_all.at[token_rows(span, lane)]
@@ -592,23 +602,25 @@
         block = norm_all.at[token_rows(span, cross)]
         return remote(block, block, diag_sem.at[span], tp=mate)
 
-    def spread_block(way, hop):
+    def spread_block(way, hop, c):
         if hop + 1 >= spans:
             return
 
         @pl.when(passes(way, hop))
         def _():
-            norm_copy(way, hop).start()
+            norm_copy(way, hop, c).start()
 
     def norm_hop(hop):
-        for way in range(2):
-
-            @pl.when(inside(origin(way, hop)))
-            def _():
-                norm_copy(way, hop - 1).wait_recv()
-                spread_block(way, hop)
-                cross_copy(clamp(origin(way, hop))).start()
-                mate_copy(clamp(origin(way, hop))).start()
+        for c in range(slabs):
+            for way in range(2):
+
+                @pl.when(inside(origin(way, hop)))
+                def _():
+                    norm_copy(way, hop - 1, c).wait_recv()
+                    spread_block(way, hop, c)
+                    if c == slabs - 1:
+                        cross_copy(clamp(origin(way, hop))).start()
+                        mate_copy(clamp(origin(way, hop))).start()
 
     def cross_hop(hop):
         for way in range(2 if hop else 1):
@@ -619,54 +631,83 @@
                 diag_copy(clamp(origin(way, hop))).start()
 
     with jax.named_scope("norm0"):
-        for way in range(2):
-            spread_block(way, 0)
+        for c in range(slabs):
+            for way in range(2):
+                spread_block(way, 0, c)
         cross_copy(me).start()
         mate_copy(me).start()
+    with jax.named_scope("relay1"):
+        relay_weights(0, 1)
+    with jax.named_scope("norm_hop1"):
+        norm_hop(1)
         start_weights(0, 3)
+    with jax.named_scope("cross0"):
+        cross_hop(0)
     with jax.named_scope("relay2"):
         relay_weights(0, 2)
-    for hop in range(1, spans):
-        with jax.named_scope("norm_hop"):
+    with jax.named_scope("norm_hop2"):
+        norm_hop(2)
+        start_weights(1, 1)
+    with jax.named_scope("cross1"):
+        cross_hop(1)
+    with jax.named_scope("relay3"):
+        relay_weights(0, 3)
+    with jax.named_scope("norm_hop3"):
+        for hop in range(3, spans):
             norm_hop(hop)
-            start_weights(1, hop)
-            cross_hop(hop - 1)
-    with jax.named_scope("norm_last"):
-        cross_hop(spans - 1)
+        start_weights(1, 2)
+        start_weights(1, 3)
+    with jax.named_scope("cross2"):
+        cross_hop(2)
+    with jax.named_scope("cross3"):
+        for hop in range(3, spans):
+            cross_hop(hop)
+    with jax.named_scope("relay_early"):
+        relay_weights(1, 1)
+    with jax.named_scope("mate_wait"):
         for span in range(spans):
             mate_copy(span).wait_recv()
             diag_copy(span).wait_recv()
-    with jax.named_scope("relay3"):
-        relay_weights(0, 3)
-        own_weights(0, False)
-        for d in range(1, spans):
-            for g in range(2):
-                relay_copy(0, d, g).wait_recv()
 
     row_at = lax.broadcasted_iota(jnp.int32, (total, 1), 0)
+
+    def twin_wait(part):
+        def step():
+            own_wait(part).wait()
+            for d in range(1, spans):
+                relay_copy(part, d).wait_recv()
+
+        when_extra(part, me, step)
 
     def compute_hidden(part):
         cols = cols_of(part, me)
-        convs = []
-        for g, taps in enumerate((gate_taps, up_taps)):
-            here = jnp.dot(norm_all[...], wides[part][g], preferred_element_type=f32)
-            here = here.astype(bf16).astype(f32)
-            earlier, later = pltpu.roll(here, 1, 0), pltpu.roll(here, total - 1, 0)
-            earlier = jnp.where(row_at == 0, 0.0, earlier)
-            later = jnp.where(row_at == total - 1, 0.0, later)
-            weight = taps[:, cols].astype(f32)
-            convs.append(weight[0:1] * earlier + weight[1:2] * here + weight[2:3] * later)
-        hidden = ((convs[0] / (1.0 + jnp.exp(-convs[0]))) * convs[1]).astype(bf16)
-        hid_all[:, cols] = hidden
+        both = jnp.dot(norm_all[...], wide[part], preferred_element_type=f32)
+        here = both.astype(bf16).astype(f32)
+        earlier, later = pltpu.roll(here, 1, 0), pltpu.roll(here, total - 1, 0)
+        earlier = jnp.where(row_at == 0, 0.0, earlier)
+        later = jnp.where(row_at == total - 1, 0.0, later)
+        weight = jnp.concatenate(
+            [gate_taps[:, cols].astype(f32), up_taps[:, cols].astype(f32)], axis=1
+        )
+        conv = weight[0:1] * earlier + weight[1:2] * here + weight[2:3] * later
+        level = conv[:, :128]
+        hid_all[:, cols] = ((level / (1.0 + jnp.exp(-level))) * conv[:, 128:]).astype(bf16)
+
+    groups = max(spans // 2, 1)
+    depth = spans // groups
+
+    def blocks(part):
+        return groups
 
     def hidden_copy(part, way, hop, b):
-        block = hid_all.at[pl.ds(b * rows, rows), cols_of(part, clamp(origin(way, hop)))]
+        size = total // blocks(part)
+        block = hid_all.at[pl.ds(b * size, size), cols_of(part, clamp(origin(way, hop)))]
         return remote(
             block, block, hid_sem.at[part, way, hop, b], sp=clamp(me + steps[way])
         )
 
     def has(part, span):
-        return inside(span) & extra(clamp(span)) if part else inside(span)
+        return inside(span) & extra(clamp(span)) if part == least else inside(span)
 
     def hidden_start(part, way, hop, b):
         if hop + 1 >= spans:
@@ -685,67 +726,80 @@
 
             hidden_start(part, way, hop, b)
 
-    with jax.named_scope("hidden_a"):
-        compute_hidden(0)
-        for b in range(spans):
-            for way in range(2):
-                hidden_start(0, way, 0, b)
-    with jax.named_scope("relay4"):
-        for d in range(1, spans):
-            relay_weights(1, d)
-    with jax.named_scope("relay5"):
-
-        @pl.when(extra(me))
-        def _():
-            for d in range(1, spans):
-                for g in range(2):
-                    relay_copy(1, d, g).wait_recv()
-
-        own_weights(1, False)
-    with jax.named_scope("hidden_b"):
-
-        @pl.when(extra(me))
-        def _():
-            compute_hidden(1)
-
-        for b in range(spans):
-            for way in range(2):
-                hidden_start(1, way, 0, b)
-    with jax.named_scope("pass_a"):
-        for hop in range(1, spans):
-            for b in range(spans):
-                hidden_pass(0, hop, b)
+    def hidden_hop(part, hop):
+        with jax.named_scope(f"pass{part}_{hop}"):
+            for b in range(blocks(part)):
+                hidden_pass(part, hop, b)
+
+    def make_hidden(part):
+        with jax.named_scope(f"twin{part}"):
+            twin_wait(part)
+        with jax.named_scope(f"hidden{part}"):
+            if part == least:
+
+                @pl.when(extra(me))
+                def _():
+                    compute_hidden(part)
+
+            else:
+                compute_hidden(part)
+            for b in range(blocks(part)):
+                for way in range(2):
+                    hidden_start(part, way, 0, b)
+
+    make_hidden(0)
+    for part in range(1, parts):
+        with jax.named_scope(f"relay_p{part}"):
+            if part + 1 < parts:
+                for d in range(1, spans):
+                    start_weights(part + 1, d)
+            for d in range(1 + (part == 1), spans):
+                relay_weights(part, d)
+        if part > 1:
+            for hop in range(2, spans):
+                hidden_hop(part - 2, hop)
+        hidden_hop(part - 1, 1)
+        make_hidden(part)
+    if parts > 1:
+        for hop in range(2, spans):
+            hidden_hop(parts - 2, hop)
     loads[7].wait()
     fans = {}
-    for b in range(spans):
+    for b in range(groups):
         with jax.named_scope("pass_b"):
             for hop in range(1, spans):
-                hidden_pass(1, hop, b)
+                hidden_pass(parts - 1, hop, b)
         with jax.named_scope("down"):
-            tp_send[b] = lax.dot_general(
-                hid_all[b * rows : (b + 1) * rows, :],
-                down_w[...],
-                (((1,), (1,)), ((), ())),
-                preferred_element_type=f32,
-            ).astype(bf16)
+            few = slice(b * depth, (b + 1) * depth)
+            tp_send[few] = (
+                lax.dot_general(
+                    hid_all[b * depth * rows : (b + 1) * depth * rows, :],
+                    down_w[...],
+                    (((1,), (1,)), ((), ())),
+                    preferred_element_type=f32,
+                )
+                .astype(bf16)
+                .reshape(depth, rows, part_cols)
+            )
             for d in range(1, shares):
                 fans[b, d] = send(
-                    tp_send.at[b, share_rows(share_at(d))],
-                    tp_recv.at[b, d],
-                    tp_sem.at[b, d],
+                    tp_send.at[pl.ds(b * depth, depth), share_rows(share_at(d))],
+                    tp_recv.at[d, pl.ds(b * depth, depth)],
+                    tp_sem.at[b, d - 1],
                     tp=share_at(d),
                 )
 
     def row_out(b):
         d = lax.rem(b - me + spans, spans)
-        return remote(row_send.at[b], row_recv.at[me], row_sem.at[d], sp=b)
+        return remote(row_send.at[b], row_recv.at[me], row_sem.at[jnp.maximum(d - 1, 0)], sp=b)
 
     for b in range(spans):
         with jax.named_scope("rows"):
             summed = tp_send[b, share_rows(lane), :].astype(f32)
             for d in range(1, shares):
-                fans[b, d].wait_recv()
-                summed = summed + tp_recv[b, d].astype(f32)
+                if b % depth == 0:
+                    fans[b // depth, d].wait_recv()
+                summed = summed + tp_recv[d, b].astype(f32)
             row_send[b] = summed.astype(bf16)
 
             @pl.when(b != me)
@@ -767,16 +821,14 @@
     with jax.named_scope("drain"):
         for copy in sends:
             copy.wait_send()
-        for part in range(2):
+        for part in range(parts):
             for d in range(1, spans):
 
                 def sent():
-                    for g in range(2):
-                        weight_copy(part, d, g).wait_send()
+                    weight_wait(part, d).wait_send()
 
                 def relayed():
-                    for g in range(2):
-                        relay_copy(part, d, g).wait_send()
+                    relay_copy(part, d).wait_send()
 
                 when_extra(part, span_at(d), sent)
                 when_extra(part, me, relayed)
@@ -794,13 +846,14 @@
 
                 @pl.when(passes(way, hop))
                 def _():
-                    norm_copy(way, hop).wait_send()
-
-                for part in range(2):
+                    for c in range(slabs):
+                        norm_copy(way, hop, c).wait_send()
+
+                for part in range(parts):
 
                     @pl.when(passes(way, hop) & has(part, origin(way, hop)))
                     def _():
-                        for b in range(spans):
+                        for b in range(blocks(part)):
                             hidden_copy(part, way, hop, b).wait_send()
 
 
@@ -827,6 +880,7 @@
     part_cols, share = (model // spans, rows // shares)
     total = spans * rows
     least, rest = tile_split(units // 128, spans)
+    parts = least + (rest > 0)
     lines = log_decay.shape[0] * log_decay.shape[1]
     heads = width // HEAD
     rates = log_decay.reshape(lines, rows)
@@ -852,30 +906,29 @@
             vmem((spans, lines, rows), f32),
             vmem((2, heads, HEAD, HEAD), bf16),
             vmem((spans, heads, HEAD, HEAD), bf16),
-            vmem((2, model, least * 128), bf16),
-            vmem((2, model, 128), bf16),
+            vmem((parts, model, 256), bf16),
             vmem((rows, model), bf16),
             vmem((shares, share, model), bf16),
             vmem((share, model), bf16),
             vmem((total, model), bf16),
             vmem((total, units), bf16),
             vmem((spans, rows, part_cols), bf16),
-            vmem((spans, shares, share, part_cols), bf16),
+            vmem((shares, spans, share, part_cols), bf16),
             vmem((spans, share, part_cols), bf16),
             vmem((spans, share, part_cols), bf16),
             dma((8,)),
-            dma((2, 2)),
-            dma((spans, 2, 2)),
-            dma((2, spans, 2, 2)),
-            dma((2, spans, 2, 2)),
-            dma((shares, 2)),
-            dma((2, spans, 2)),
+            dma((parts,)),
+            dma((spans - 1, 2, 2)),
+            dma((parts, spans - 1, 2)),
+            dma((parts, spans - 1, 2)),
+            dma((shares - 1, 2)),
+            dma((2, spans - 1, 2, 2)),
             dma((spans, 2)),
             dma((spans, 2)),
             dma((spans, 2)),
-            dma((2, 2, spans, spans, 2)),
-            dma((spans, shares, 2)),
-            dma((spans, 2)),
+            dma((parts, 2, spans - 1, spans // 2, 2)),
+            dma((spans // 2, shares - 1, 2)),
+            dma((spans - 1, 2)),
         ],
         compiler_params=pltpu.CompilerParams(collective_id=0, has_side_effects=True),
     )(
@@ -886,7 +939,7 @@
         rates,
         head_gain,
         residual,
-        norm_gain.reshape(1, model),
+        norm_gain.reshape(model // 128, 128),
         gate_taps,
         up_taps,
         out_weight,
@@ -901,7 +954,8 @@
     span_tokens = args[0].shape[0] * spans
     model_width = args[7].shape[1]
     lanes = args[9].shape[1] // 128
-    if span_tokens < model_width and twins == 2 and shares == 4 and lanes >= spans:
+    even = spans % 2 == 0 and lanes >= spans
+    if even and span_tokens < model_width and twins == 2 and shares == 4:
         return fused_block(*args)
     return shards(*args)
 

time: 103 us -> 88.2 us (0.86)
  Pallas kernels: 99.6 us -> 86.2 us
  local copies, waits for them, and re-layouts: 2.86 us -> 1.57 us
    pallas_call x1, Pallas kernels: 99.6 us -> 86.2 us  [fused_block(): pl.pallas_call(functools.partial(block_kernel, spans, shares), out_shape=...]
    reshape x1 -> x0, local copies, waits for them, and re-layouts: 1.29 us -> none  [fused_block(): norm_gain.reshape(1, model)]
where the time goes in v2:
time: 88.2 us; the launch traced here: 87.8 us
  Pallas kernels  86.2 us (98%)
  local copies, waits for them, and re-layouts  1.57 us (2%)
    pallas_call x1, Pallas kernels, fused_block(): pl.pallas_call(functools.partial(block_kernel, spans, shares), out_shape=...  86.2 us

profile of v2, /device:TPU:0, one launch (start us, length us, event | category | flops | bytes accessed | tf_op | source)
XLA Modules:
  0.0 87.8 jit_solution(1842156888357331376)
XLA Ops:
  0.0 86.2 %shard_map.136 = bf16[32,2048]{1,0:T(8,128)(2,1)} custom-call(bf16[128,256]{1,0:T(8,128)(2,1)} %query_hbm.1, bf16[128,256]{1,0:T(8,128)(2,1)} %key_hbm.1, bf16[128,256]{1,0:T(8,128)(2,1)} %value_hbm.1, bf16[128,256]{1,0:T(8,128)(2,1)} %gate_hbm.1, f32[4,128]{1,0:T(4,128)} %bitcast.3, f32[2,256]{1,0:T(2,128)} %gains.1, bf16[128,2048]{1,0:T(8,128)(2,1)} %residual_hbm.1, ...), custom_call_target="tpu_custom_call" | custom-call | tf_op jit(solution)/shard_map/pallas_call | solution.py:892
  86.2 1.6 %copy.16 = bf16[32,2048]{1,0:T(8,128)(2,1)} copy(bf16[32,2048]{1,0:T(8,128)(2,1)} %shard_map.136) | data formatting | bytes 262144

commit v3 on v2

--- a/solution.py
+++ b/solution.py
@@ -9,6 +9,11 @@
 from jax.sharding import PartitionSpec as P
 
 HEAD = 128
+GRANT = 40 << 20
+SLABS = 4
+EARLY = ((0, 3), (0, 1), (0, 2))
+SECOND = ()
+ORDER = (('r', 0, 1), ('n', 1), ('x', 0), ('r', 0, 2), ('n', 2), ('w', 1, 1), ('x', 1), ('r', 0, 3), ('w', 1, 2), ('w', 1, 3), ('n', 3), ('x', 2), ('x', 3), ('r', 1, 1), ('m',), ('H', 0), ('w', 2, 1), ('w', 2, 2), ('w', 2, 3), ('r', 1, 2), ('r', 1, 3), ('h', 0, 1, 0), ('h', 0, 1, 1), ('H', 1), ('r', 2, 1), ('r', 2, 2), ('r', 2, 3), ('h', 0, 2, 0), ('h', 0, 2, 1), ('h', 0, 3, 0), ('h', 0, 3, 1), ('h', 1, 1, 0), ('h', 1, 1, 1), ('H', 2), ('h', 1, 2, 0), ('h', 1, 2, 1), ('h', 1, 3, 0), ('h', 1, 3, 1), ('h', 2, 1, 0), ('h', 2, 2, 0), ('h', 2, 3, 0), ('D', 0), ('h', 2, 1, 1), ('h', 2, 2, 1), ('h', 2, 3, 1), ('D', 1), ('P', 0), ('P', 1), ('R', 0), ('R', 1))
 
 
 FULL_PRECISION = lax.Precision.HIGHEST
@@ -210,11 +215,11 @@
     value_hbm,
     gate_hbm,
     rates_hbm,
-    gains,
+    gains_hbm,
     residual_hbm,
-    norm_gain,
-    gate_taps,
-    up_taps,
+    norm_gain_hbm,
+    gate_taps_hbm,
+    up_taps_hbm,
     out_hbm,
     fg_hbm,
     fu_hbm,
@@ -228,32 +233,45 @@
     residual,
     out_w,
     down_w,
+    gains,
+    norm_gain,
+    gate_taps,
+    up_taps,
     rate_all,
     state_send,
     state_recv,
     wide,
     att_send,
     att_recv,
+    att_mid,
     middle_ref,
     norm_all,
     hid_all,
     tp_send,
     tp_recv,
+    tp_mid,
     row_send,
     row_recv,
     local_sem,
     own_sem,
     state_sem,
+    state_leave,
     w_sem,
     relay_sem,
+    w_leave,
+    relay_leave,
     att_sem,
     norm_sem,
-    mate_sem,
+    norm_leave,
     cross_sem,
-    diag_sem,
+    gather_sem,
+    leave_sem,
     hid_sem,
+    hid_leave,
     tp_sem,
+    tp_leave,
     row_sem,
+    row_leave,
 ):
     side, me, lane = lax.axis_index("grp"), lax.axis_index("sp"), lax.axis_index("tp")
     rows, width = query.shape
@@ -271,14 +289,15 @@
     mate = lane + 1 - 2 * lax.rem(lane, 2)
     cross = lax.rem(lane + shares // 2, shares)
     odd = lax.rem(lane, 2)
+    diag = cross + 1 - 2 * odd
     sends = []
 
-    def remote(src, dst, sems, **place):
+    def remote(src, dst, sems, leave=None, **place):
         return pltpu.make_async_remote_copy(
             src_ref=src,
             dst_ref=dst,
-            send_sem=sems.at[0],
-            recv_sem=sems.at[1],
+            send_sem=sems.at[0] if leave is None else leave,
+            recv_sem=sems.at[1] if leave is None else sems,
             device_id=place,
             device_id_type=pl.DeviceIdType.MESH,
         )
@@ -328,6 +347,10 @@
                 (out_hbm, out_w),
                 (residual_hbm, residual),
                 (down_hbm, down_w),
+                (gains_hbm, gains),
+                (norm_gain_hbm, norm_gain),
+                (gate_taps_hbm, gate_taps),
+                (up_taps_hbm, up_taps),
             )
         )
     ]
@@ -353,6 +376,9 @@
     def half_rows(span):
         begin = span * part_cols + side * half
         return pl.ds(pl.multiple_of(begin, half), half)
+
+    def leave_at(part, d):
+        return part if part < least else least + d - 1
 
     def weight_copy(part, d, g):
         to = span_at(d)
@@ -360,16 +386,18 @@
             weights[g].at[pl.ds(pl.multiple_of(side * half, half), half), cols_of(part, to)],
             wide.at[part, half_rows(me), lanes(g)],
             w_sem.at[part, d - 1],
+            w_leave.at[leave_at(part, d)],
             sp=to,
         )
 
     def relay_copy(part, d):
         block = wide.at[part, half_rows(lax.rem(me + spans - d, spans))]
-        return remote(block, block, relay_sem.at[part, d - 1], grp=1 - side)
+        return remote(block, block, relay_sem.at[part, d - 1], relay_leave.at[part], grp=1 - side)
 
     def weight_wait(part, d):
         block = wide.at[part, half_rows(lax.rem(me + spans - d, spans))]
-        return remote(block, block, w_sem.at[part, d - 1], sp=span_at(d))
+        sem = w_sem.at[part, d - 1]
+        return remote(block, block, sem, w_leave.at[leave_at(part, d)], sp=span_at(d))
 
     def when_extra(part, span, step):
         if part == least:
@@ -453,10 +481,21 @@
     for d in range(1, spans):
         to = span_at(d)
         way = jnp.where(to > me, 0, 1)
-        arrivals.append(send(rates, rate_all.at[me], state_sem.at[d - 1, 0], sp=to))
         arrivals.append(
-            send(state_send.at[way], state_recv.at[me], state_sem.at[d - 1, 1], sp=to)
-        )
+            remote(rates, rate_all.at[me], state_sem.at[d - 1, 0], state_leave.at[0], sp=to)
+        )
+        arrivals.append(
+            remote(
+                state_send.at[way],
+                state_recv.at[me],
+                state_sem.at[d - 1, 1],
+                state_leave.at[1],
+                sp=to,
+            )
+        )
+    for copy in arrivals:
+        copy.start()
+
     with jax.named_scope("inner"):
         loads[3].wait()
         inner = []
@@ -484,8 +523,10 @@
         for copy in arrivals:
             copy.wait_recv()
         loads[4].wait()
-        start_weights(0, 1)
-        start_weights(0, 2)
+        for load in loads[8:]:
+            load.wait()
+        for part, d in EARLY:
+            start_weights(part, d)
     with jax.named_scope("outer"):
         sums = [jnp.sum(rate_all[j], axis=1, keepdims=True) for j in range(spans)]
         mixed = []
@@ -534,27 +575,30 @@
             att_send[:, at : at + step_cols] = jnp.dot(
                 mixed, out_w[:, at : at + step_cols], preferred_element_type=f32
             ).astype(bf16)
-        arrivals = [
-            send(
-                att_send.at[share_rows(share_at(d))],
-                att_recv.at[d],
-                att_sem.at[d - 1],
-                tp=share_at(d),
-            )
-            for d in range(1, shares)
+        pairs = [
+            send(att_send.at[share_rows(to)], att_recv.at[i], att_sem.at[i], tp=mate)
+            for i, to in enumerate((diag, mate))
         ]
+    for part, d in SECOND:
+        start_weights(part, d)
+    with jax.named_scope("attended_pair"):
+        loads[6].wait()
+        pairs[0].wait_recv()
+        att_mid[...] = (
+            att_send[share_rows(cross), :].astype(f32) + att_recv[0].astype(f32)
+        ).astype(bf16)
+        pairs.append(send(att_mid, att_recv.at[2], att_sem.at[2], tp=cross))
+        pairs[1].wait_recv()
     with jax.named_scope("attended_wait"):
-        loads[6].wait()
-        for copy in arrivals:
-            copy.wait_recv()
+        pairs[2].wait_recv()
 
     def token_rows(span, tp):
         return pl.ds(pl.multiple_of(span * rows + tp * share, share), share)
 
     with jax.named_scope("normed"):
         attended = att_send[share_rows(lane), :].astype(f32)
-        for d in range(1, shares):
-            attended = attended + att_recv[d].astype(f32)
+        for i in range(1, 3):
+            attended = attended + att_recv[i].astype(f32)
         middle = (residual[share_rows(lane), :].astype(f32) + attended).astype(bf16)
         middle_ref[...] = middle
         middle = middle.astype(f32)
@@ -579,28 +623,27 @@
     def passes(way, hop):
         return inside(origin(way, hop)) & inside(me + steps[way])
 
-    slabs = 2
-    slab = share // slabs
-
-    def slab_rows(span, tp, c):
-        begin = span * rows + tp * share + c * slab
-        return pl.ds(pl.multiple_of(begin, slab), slab)
+    slab = model // SLABS
+
+    def slab_of(span, tp, c):
+        return norm_all.at[token_rows(span, tp), c * slab : (c + 1) * slab]
 
     def norm_copy(way, hop, c):
-        block = norm_all.at[slab_rows(clamp(origin(way, hop)), lane, c)]
-        return remote(block, block, norm_sem.at[way, hop, c], sp=clamp(me + steps[way]))
-
-    def mate_copy(span):
-        block = norm_all.at[token_rows(span, lane)]
-        return remote(block, block, mate_sem.at[span], tp=mate)
-
-    def cross_copy(span):
-        block = norm_all.at[token_rows(span, lane)]
-        return remote(block, block, cross_sem.at[span], tp=cross)
-
-    def diag_copy(span):
-        block = norm_all.at[token_rows(span, cross)]
-        return remote(block, block, diag_sem.at[span], tp=mate)
+        block = slab_of(clamp(origin(way, hop)), lane, c)
+        to = clamp(me + steps[way])
+        return remote(block, block, norm_sem.at[way, hop, c], norm_leave.at[way, hop], sp=to)
+
+    def mate_copy(span, c):
+        block = slab_of(span, lane, c)
+        return remote(block, block, gather_sem.at[0], leave_sem.at[0], tp=mate)
+
+    def cross_copy(span, c):
+        block = slab_of(span, lane, c)
+        return remote(block, block, cross_sem.at[span, c], leave_sem.at[1], tp=cross)
+
+    def diag_copy(span, c):
+        block = slab_of(span, cross, c)
+        return remote(block, block, gather_sem.at[1], leave_sem.at[2], tp=mate)
 
     def spread_block(way, hop, c):
         if hop + 1 >= spans:
@@ -611,63 +654,35 @@
             norm_copy(way, hop, c).start()
 
     def norm_hop(hop):
-        for c in range(slabs):
+        for c in range(SLABS):
             for way in range(2):
 
                 @pl.when(inside(origin(way, hop)))
                 def _():
                     norm_copy(way, hop - 1, c).wait_recv()
                     spread_block(way, hop, c)
-                    if c == slabs - 1:
-                        cross_copy(clamp(origin(way, hop))).start()
-                        mate_copy(clamp(origin(way, hop))).start()
+                    cross_copy(clamp(origin(way, hop)), c).start()
+                    mate_copy(clamp(origin(way, hop)), c).start()
 
     def cross_hop(hop):
         for way in range(2 if hop else 1):
 
             @pl.when(inside(origin(way, hop)))
             def _():
-                cross_copy(clamp(origin(way, hop))).wait_recv()
-                diag_copy(clamp(origin(way, hop))).start()
+                for c in range(SLABS):
+                    cross_copy(clamp(origin(way, hop)), c).wait_recv()
+                    diag_copy(clamp(origin(way, hop)), c).start()
 
     with jax.named_scope("norm0"):
-        for c in range(slabs):
+        for c in range(SLABS):
             for way in range(2):
                 spread_block(way, 0, c)
-        cross_copy(me).start()
-        mate_copy(me).start()
-    with jax.named_scope("relay1"):
-        relay_weights(0, 1)
-    with jax.named_scope("norm_hop1"):
-        norm_hop(1)
-        start_weights(0, 3)
-    with jax.named_scope("cross0"):
-        cross_hop(0)
-    with jax.named_scope("relay2"):
-        relay_weights(0, 2)
-    with jax.named_scope("norm_hop2"):
-        norm_hop(2)
-        start_weights(1, 1)
-    with jax.named_scope("cross1"):
-        cross_hop(1)
-    with jax.named_scope("relay3"):
-        relay_weights(0, 3)
-    with jax.named_scope("norm_hop3"):
-        for hop in range(3, spans):
-            norm_hop(hop)
-        start_weights(1, 2)
-        start_weights(1, 3)
-    with jax.named_scope("cross2"):
-        cross_hop(2)
-    with jax.named_scope("cross3"):
-        for hop in range(3, spans):
-            cross_hop(hop)
-    with jax.named_scope("relay_early"):
-        relay_weights(1, 1)
-    with jax.named_scope("mate_wait"):
-        for span in range(spans):
-            mate_copy(span).wait_recv()
-            diag_copy(span).wait_recv()
+            cross_copy(me, c).start()
+            mate_copy(me, c).start()
+    def gather_wait():
+        whole = norm_all.at[pl.ds(0, rows)]
+        for i in range(2):
+            remote(whole, whole, gather_sem.at[i], leave_sem.at[0], tp=mate).wait_recv()
 
     row_at = lax.broadcasted_iota(jnp.int32, (total, 1), 0)
 
@@ -703,7 +718,11 @@
         size = total // blocks(part)
         block = hid_all.at[pl.ds(b * size, size), cols_of(part, clamp(origin(way, hop)))]
         return remote(
-            block, block, hid_sem.at[part, way, hop, b], sp=clamp(me + steps[way])
+            block,
+            block,
+            hid_sem.at[part, way, hop, b],
+            hid_leave.at[part, way, hop],
+            sp=clamp(me + steps[way]),
         )
 
     def has(part, span):
@@ -726,80 +745,77 @@
 
             hidden_start(part, way, hop, b)
 
-    def hidden_hop(part, hop):
-        with jax.named_scope(f"pass{part}_{hop}"):
-            for b in range(blocks(part)):
-                hidden_pass(part, hop, b)
-
     def make_hidden(part):
-        with jax.named_scope(f"twin{part}"):
-            twin_wait(part)
-        with jax.named_scope(f"hidden{part}"):
-            if part == least:
-
-                @pl.when(extra(me))
-                def _():
-                    compute_hidden(part)
-
-            else:
+        twin_wait(part)
+        if part == least:
+
+            @pl.when(extra(me))
+            def _():
                 compute_hidden(part)
-            for b in range(blocks(part)):
-                for way in range(2):
-                    hidden_start(part, way, 0, b)
-
-    make_hidden(0)
-    for part in range(1, parts):
-        with jax.named_scope(f"relay_p{part}"):
-            if part + 1 < parts:
-                for d in range(1, spans):
-                    start_weights(part + 1, d)
-            for d in range(1 + (part == 1), spans):
-                relay_weights(part, d)
-        if part > 1:
-            for hop in range(2, spans):
-                hidden_hop(part - 2, hop)
-        hidden_hop(part - 1, 1)
-        make_hidden(part)
-    if parts > 1:
-        for hop in range(2, spans):
-            hidden_hop(parts - 2, hop)
-    loads[7].wait()
-    fans = {}
-    for b in range(groups):
-        with jax.named_scope("pass_b"):
-            for hop in range(1, spans):
-                hidden_pass(parts - 1, hop, b)
-        with jax.named_scope("down"):
-            few = slice(b * depth, (b + 1) * depth)
-            tp_send[few] = (
-                lax.dot_general(
-                    hid_all[b * depth * rows : (b + 1) * depth * rows, :],
-                    down_w[...],
-                    (((1,), (1,)), ((), ())),
-                    preferred_element_type=f32,
-                )
-                .astype(bf16)
-                .reshape(depth, rows, part_cols)
+
+        else:
+            compute_hidden(part)
+        for b in range(blocks(part)):
+            for way in range(2):
+                hidden_start(part, way, 0, b)
+
+    pairs, crossing = {}, {}
+
+    def down(b):
+        few = pl.ds(b * depth, depth)
+        if b == 0:
+            loads[7].wait()
+        tp_send[few] = (
+            lax.dot_general(
+                hid_all[b * depth * rows : (b + 1) * depth * rows, :],
+                down_w[...],
+                (((1,), (1,)), ((), ())),
+                preferred_element_type=f32,
             )
-            for d in range(1, shares):
-                fans[b, d] = send(
-                    tp_send.at[pl.ds(b * depth, depth), share_rows(share_at(d))],
-                    tp_recv.at[d, pl.ds(b * depth, depth)],
-                    tp_sem.at[b, d - 1],
-                    tp=share_at(d),
-                )
+            .astype(bf16)
+            .reshape(depth, rows, part_cols)
+        )
+        pairs[b] = [
+            remote(
+                tp_send.at[few, share_rows(to)],
+                tp_recv.at[i, few],
+                tp_sem.at[b, i],
+                tp_leave.at[0],
+                tp=mate,
+            )
+            for i, to in enumerate((diag, mate))
+        ]
+        for copy in pairs[b]:
+            copy.start()
+
+    def cross_step(b):
+        few = pl.ds(b * depth, depth)
+        pairs[b][0].wait_recv()
+        tp_mid[few] = (
+            tp_send[few, share_rows(cross)].astype(f32) + tp_recv[0, few].astype(f32)
+        ).astype(bf16)
+        crossing[b] = remote(
+            tp_mid.at[few], tp_recv.at[2, few], tp_sem.at[b, 2], tp_leave.at[0], tp=cross
+        )
+        crossing[b].start()
+        pairs[b][1].wait_recv()
 
     def row_out(b):
         d = lax.rem(b - me + spans, spans)
-        return remote(row_send.at[b], row_recv.at[me], row_sem.at[jnp.maximum(d - 1, 0)], sp=b)
-
-    for b in range(spans):
-        with jax.named_scope("rows"):
+        return remote(
+            row_send.at[b],
+            row_recv.at[me],
+            row_sem.at[jnp.maximum(d - 1, 0)],
+            row_leave.at[0],
+            sp=b,
+        )
+
+    def row_step(group):
+        crossing[group].wait_recv()
+        for b in range(group * depth, (group + 1) * depth):
             summed = tp_send[b, share_rows(lane), :].astype(f32)
-            for d in range(1, shares):
-                if b % depth == 0:
-                    fans[b // depth, d].wait_recv()
-                summed = summed + tp_recv[d, b].astype(f32)
+            for i in range(1, 3):
+                summed = summed + tp_recv[i, b].astype(f32)
             row_send[b] = summed.astype(bf16)
 
             @pl.when(b != me)
@@ -809,6 +825,22 @@
             @pl.when(b == me)
             def _():
                 row_recv[me] = row_send[b]
+
+    actions = {
+        "n": norm_hop,
+        "x": cross_hop,
+        "w": start_weights,
+        "r": relay_weights,
+        "m": gather_wait,
+        "H": make_hidden,
+        "h": hidden_pass,
+        "D": down,
+        "P": cross_step,
+        "R": row_step,
+    }
+    for name, *numbers in ORDER:
+        with jax.named_scope(name + "".join(str(number) for number in numbers)):
+            actions[name](*numbers)
 
     with jax.named_scope("final"):
         for d in range(1, spans):
@@ -822,39 +854,61 @@
         for copy in sends:
             copy.wait_send()
         for part in range(parts):
-            for d in range(1, spans):
+            if part < least:
+                block = wide.at[part, pl.ds(0, (spans - 1) * half)]
+                remote(
+                    block, block, w_sem.at[part, 0], w_leave.at[part], sp=span_at(1)
+                ).wait_send()
+            for d in range(1, spans if part == least else 1):
 
                 def sent():
                     weight_wait(part, d).wait_send()
 
-                def relayed():
-                    relay_copy(part, d).wait_send()
-
                 when_extra(part, span_at(d), sent)
-                when_extra(part, me, relayed)
-        for span in range(spans):
-            cross_copy(span).wait_send()
-            mate_copy(span).wait_send()
-            diag_copy(span).wait_send()
-
-            @pl.when(span != me)
-            def _():
-                row_out(span).wait_send()
-
+
+            def relayed():
+                block = wide.at[part, pl.ds(0, (spans - 1) * half)]
+                remote(
+                    block, block, relay_sem.at[part, 0], relay_leave.at[part], grp=1 - side
+                ).wait_send()
+
+            when_extra(part, me, relayed)
+        whole = norm_all.at[pl.ds(0, rows)]
+        for i in range(3):
+            remote(whole, whole, gather_sem.at[0], leave_sem.at[i], tp=mate).wait_send()
+        remote(state_recv.at[pl.ds(0, spans - 1)], state_recv.at[pl.ds(0, spans - 1)],
+               state_sem.at[0, 1], state_leave.at[1], sp=span_at(1)).wait_send()
+        remote(rate_all.at[pl.ds(0, spans - 1)], rate_all.at[pl.ds(0, spans - 1)],
+               state_sem.at[0, 0], state_leave.at[0], sp=span_at(1)).wait_send()
+        remote(tp_recv, tp_recv, tp_sem.at[0, 0], tp_leave.at[0], tp=mate).wait_send()
+        remote(row_recv.at[pl.ds(0, spans - 1)], row_recv.at[pl.ds(0, spans - 1)],
+               row_sem.at[0], row_leave.at[0], sp=span_at(1)).wait_send()
         for way in range(2):
             for hop in range(spans - 1):
 
                 @pl.when(passes(way, hop))
                 def _():
-                    for c in range(slabs):
-                        norm_copy(way, hop, c).wait_send()
+                    block = norm_all.at[pl.ds(0, share)]
+                    remote(
+                        block,
+                        block,
+                        norm_sem.at[way, hop, 0],
+                        norm_leave.at[way, hop],
+                        sp=clamp(me + steps[way]),
+                    ).wait_send()
 
                 for part in range(parts):
 
                     @pl.when(passes(way, hop) & has(part, origin(way, hop)))
                     def _():
-                        for b in range(blocks(part)):
-                            hidden_copy(part, way, hop, b).wait_send()
+                        block = hid_all.at[:, pl.ds(0, 128)]
+                        remote(
+                            block,
+                            block,
+                            hid_sem.at[part, way, hop, 0],
+                            hid_leave.at[part, way, hop],
+                            sp=clamp(me + steps[way]),
+                        ).wait_send()
 
 
 def fused_block(
@@ -885,14 +939,13 @@
     heads = width // HEAD
     rates = log_decay.reshape(lines, rows)
     f32, bf16 = jnp.float32, jnp.bfloat16
-    far = pl.BlockSpec(memory_space=pl.ANY)
-    near = pl.BlockSpec(memory_space=pltpu.VMEM)
+    far = pl.BlockSpec(memory_space=pltpu.HBM)
     dma = pltpu.SemaphoreType.DMA
     vmem = pltpu.VMEM
     return pl.pallas_call(
         functools.partial(block_kernel, spans, shares),
         out_shape=jax.ShapeDtypeStruct((share, model), bf16),
-        in_specs=[far] * 5 + [near, far] + [near] * 3 + [far] * 4,
+        in_specs=[far] * 14,
         out_specs=pl.BlockSpec(memory_space=pltpu.VMEM),
         scratch_shapes=[
             vmem((rows, width), bf16),
@@ -903,49 +956,69 @@
             vmem((rows, model), bf16),
             vmem(out_weight.shape, bf16),
             vmem(down_weight.shape, bf16),
+            vmem(head_gain.shape, f32),
+            vmem((model // 128, 128), bf16),
+            vmem(gate_taps.shape, bf16),
+            vmem(up_taps.shape, bf16),
             vmem((spans, lines, rows), f32),
             vmem((2, heads, HEAD, HEAD), bf16),
             vmem((spans, heads, HEAD, HEAD), bf16),
             vmem((parts, model, 256), bf16),
             vmem((rows, model), bf16),
-            vmem((shares, share, model), bf16),
+            vmem((3, share, model), bf16),
+            vmem((share, model), bf16),
             vmem((share, model), bf16),
             vmem((total, model), bf16),
             vmem((total, units), bf16),
             vmem((spans, rows, part_cols), bf16),
-            vmem((shares, spans, share, part_cols), bf16),
+            vmem((3, spans, share, part_cols), bf16),
             vmem((spans, share, part_cols), bf16),
             vmem((spans, share, part_cols), bf16),
-            dma((8,)),
+            vmem((spans, share, part_cols), bf16),
+            dma((12,)),
             dma((parts,)),
-            dma((spans - 1, 2, 2)),
-            dma((parts, spans - 1, 2)),
-            dma((parts, spans - 1, 2)),
-            dma((shares - 1, 2)),
-            dma((2, spans - 1, 2, 2)),
-            dma((spans, 2)),
-            dma((spans, 2)),
-            dma((spans, 2)),
-            dma((parts, 2, spans - 1, spans // 2, 2)),
-            dma((spans // 2, shares - 1, 2)),
             dma((spans - 1, 2)),
+            dma((2,)),
+            dma((parts, spans - 1)),
+            dma((parts, spans - 1)),
+            dma((least + spans - 1,)),
+            dma((parts,)),
+            dma((3, 2)),
+            dma((2, spans - 1, SLABS)),
+            dma((2, spans - 1)),
+            dma((spans, SLABS)),
+            dma((2,)),
+            dma((3,)),
+            dma((parts, 2, spans - 1, spans // 2)),
+            dma((parts, 2, spans - 1)),
+            dma((spans // 2, 3)),
+            dma((1,)),
+            dma((spans - 1,)),
+            dma((1,)),
         ],
-        compiler_params=pltpu.CompilerParams(collective_id=0, has_side_effects=True),
+        compiler_params=pltpu.CompilerParams(
+            collective_id=0, has_side_effects=True, vmem_limit_bytes=GRANT
+        ),
     )(
-        query_rows,
-        key_rows,
-        value_rows,
-        gate_rows,
-        rates,
-        head_gain,
-        residual,
-        norm_gain.reshape(model // 128, 128),
-        gate_taps,
-        up_taps,
-        out_weight,
-        gate_weight,
-        up_weight,
-        down_weight,
+        *(
+            pltpu.with_memory_space_constraint(value, pltpu.HBM)
+            for value in (
+                query_rows,
+                key_rows,
+                value_rows,
+                gate_rows,
+                rates,
+                head_gain,
+                residual,
+                norm_gain.reshape(model // 128, 128),
+                gate_taps,
+                up_taps,
+                out_weight,
+                gate_weight,
+                up_weight,
+                down_weight,
+            )
+        )
     )
 
 
@@ -954,8 +1027,8 @@
     span_tokens = args[0].shape[0] * spans
     model_width = args[7].shape[1]
     lanes = args[9].shape[1] // 128
-    even = spans % 2 == 0 and lanes >= spans
-    if even and span_tokens < model_width and twins == 2 and shares == 4:
+    fits = spans == 4 and lanes >= 2 * spans
+    if fits and span_tokens < model_width and twins == 2 and shares == 4:
         return fused_block(*args)
     return shards(*args)
 

time: 88.2 us -> 84.1 us (0.954)
  Pallas kernels: 86.2 us -> 83.3 us
  local copies, waits for them, and re-layouts: 1.57 us -> 0.66 us
    pallas_call x1, Pallas kernels: 86.2 us -> 83.3 us  [fused_block(): pl.pallas_call(functools.partial(block_kernel, spans, shares), out_shape=...]
    unnamed x1, local copies, waits for them, and re-layouts: 1.57 us -> 0.66 us
where the time goes in v3:
time: 84.1 us; the launch traced here: 83.9 us
  Pallas kernels  83.3 us (99%)
    pallas_call x1, Pallas kernels, fused_block(): pl.pallas_call(functools.partial(block_kernel, spans, shares), out_shape=...  83.3 us

profile of v3, /device:TPU:0, one launch (start us, length us, event | category | flops | bytes accessed | tf_op | source)
XLA Modules:
  0.0 83.9 jit_solution(18156251623463109024)
XLA Ops:
  0.0 83.3 %shard_map.136 = bf16[32,2048]{1,0:T(8,128)(2,1)S(1)} custom-call(bf16[128,256]{1,0:T(8,128)(2,1)} %query_hbm.1, bf16[128,256]{1,0:T(8,128)(2,1)} %key_hbm.1, bf16[128,256]{1,0:T(8,128)(2,1)} %value_hbm.1, bf16[128,256]{1,0:T(8,128)(2,1)} %gate_hbm.1, f32[4,128]{1,0:T(4,128)} %bitcast.3, f32[2,256]{1,0:T(2,128)} %gains_hbm.1, ...), custom_call_target="tpu_custom_call" | custom-call | tf_op jit(solution)/shard_map/pallas_call | solution.py:945
  83.3 0.7 copy.16

commit v4 on v3

--- a/solution.py
+++ b/solution.py
@@ -11,9 +11,12 @@
 HEAD = 128
 GRANT = 40 << 20
 SLABS = 4
+PAIRED = False
+SPLIT = 'even'
+WAYS = (0, 1)
 EARLY = ((0, 3), (0, 1), (0, 2))
 SECOND = ()
-ORDER = (('r', 0, 1), ('n', 1), ('x', 0), ('r', 0, 2), ('n', 2), ('w', 1, 1), ('x', 1), ('r', 0, 3), ('w', 1, 2), ('w', 1, 3), ('n', 3), ('x', 2), ('x', 3), ('r', 1, 1), ('m',), ('H', 0), ('w', 2, 1), ('w', 2, 2), ('w', 2, 3), ('r', 1, 2), ('r', 1, 3), ('h', 0, 1, 0), ('h', 0, 1, 1), ('H', 1), ('r', 2, 1), ('r', 2, 2), ('r', 2, 3), ('h', 0, 2, 0), ('h', 0, 2, 1), ('h', 0, 3, 0), ('h', 0, 3, 1), ('h', 1, 1, 0), ('h', 1, 1, 1), ('H', 2), ('h', 1, 2, 0), ('h', 1, 2, 1), ('h', 1, 3, 0), ('h', 1, 3, 1), ('h', 2, 1, 0), ('h', 2, 2, 0), ('h', 2, 3, 0), ('D', 0), ('h', 2, 1, 1), ('h', 2, 2, 1), ('h', 2, 3, 1), ('D', 1), ('P', 0), ('P', 1), ('R', 0), ('R', 1))
+ORDER = (('r', 0, 1), ('n', 1), ('x', 0), ('r', 0, 2), ('n', 2), ('w', 1, 1), ('x', 1), ('r', 0, 3), ('w', 1, 2), ('w', 1, 3), ('n', 3), ('x', 2), ('r', 1, 1), ('x', 3), ('m',), ('H', 0), ('w', 2, 1), ('r', 1, 3), ('w', 2, 2), ('r', 1, 2), ('w', 2, 3), ('h', 0, 1, 0), ('h', 0, 1, 1), ('H', 1), ('r', 2, 1), ('r', 2, 2), ('r', 2, 3), ('h', 0, 2, 0), ('h', 0, 2, 1), ('h', 0, 3, 0), ('h', 0, 3, 1), ('h', 1, 1, 0), ('h', 1, 1, 1), ('H', 2), ('h', 1, 2, 0), ('h', 1, 2, 1), ('h', 1, 3, 0), ('h', 1, 3, 1), ('h', 2, 1, 0), ('h', 2, 2, 0), ('h', 2, 3, 0), ('D', 0), ('h', 2, 1, 1), ('P', 0), ('h', 2, 2, 1), ('h', 2, 3, 1), ('D', 1), ('R', 0), ('P', 1), ('R', 1))
 
 
 FULL_PRECISION = lax.Precision.HIGHEST
@@ -202,9 +205,19 @@
     return (middle_own.astype(jnp.float32) + ff_out).astype(jnp.bfloat16)
 
 
-def tile_split(lanes, spans):
-    least, rest = divmod(lanes, spans)
-    return least, rest
+def tile_counts(lanes, spans):
+    if SPLIT == "ends":
+        outer = lanes // spans
+        near = (lanes - 2 * outer + 1) // 2
+        far = lanes - 2 * outer - near
+        even, odd = (outer, near, far, outer), (outer, far, near, outer)
+    else:
+        least, rest = divmod(lanes, spans)
+        even = tuple(least + (j < rest) for j in range(spans))
+        odd = even[::-1]
+        if SPLIT == "middle":
+            even, odd = (even[0], even[1], even[3], even[2]), (odd[1], odd[0], odd[2], odd[3])
+    return even, odd
 
 
 def block_kernel(
@@ -283,8 +296,8 @@
     total = spans * rows
     lines = rates.shape[0]
     units = gate_taps.shape[1]
-    least, rest = tile_split(units // 128, spans)
-    parts = least + (rest > 0)
+    counts = tile_counts(units // 128, spans)
+    least, parts = min(counts[0]), max(counts[0])
     f32, bf16 = jnp.float32, jnp.bfloat16
     mate = lane + 1 - 2 * lax.rem(lane, 2)
     cross = lax.rem(lane + shares // 2, shares)
@@ -311,17 +324,33 @@
     def span_at(step):
         return lax.rem(me + step, spans)
 
+    def target(d):
+        if not PAIRED:
+            return span_at(d)
+        if d == 1:
+            return me + 1 - 2 * lax.rem(me, 2)
+        return lax.rem(me + 2, spans) if d == 2 else spans - 1 - me
+
+    def source(d):
+        return target(d) if PAIRED else lax.rem(me + spans - d, spans)
+
     def share_at(step):
         return lax.rem(lane + step, shares)
 
-    def extra(span):
-        return jnp.where(odd == 0, span < rest, span >= spans - rest)
+    def pick(tables, span):
+        value = 0
+        for j in range(spans):
+            mine = jnp.where(odd == 0, tables[0][j], tables[1][j])
+            value = value + jnp.where(span == j, mine, 0)
+        return value
+
+    def holds(part, span):
+        return pick(counts, span) > part
+
+    starts = [[sum(row[:j]) for j in range(spans)] for row in counts]
 
     def first_col(span):
-        before = jnp.where(
-            odd == 0, jnp.minimum(span, rest), jnp.maximum(span - (spans - rest), 0)
-        )
-        return (span * least + before) * 128
+        return pick(starts, span) * 128
 
     def cols_of(part, span):
         begin = jnp.minimum(first_col(span) + part * 128, units - 128)
@@ -378,10 +407,10 @@
         return pl.ds(pl.multiple_of(begin, half), half)
 
     def leave_at(part, d):
-        return part if part < least else least + d - 1
+        return part if part < least else least + (part - least) * (spans - 1) + d - 1
 
     def weight_copy(part, d, g):
-        to = span_at(d)
+        to = target(d)
         return remote(
             weights[g].at[pl.ds(pl.multiple_of(side * half, half), half), cols_of(part, to)],
             wide.at[part, half_rows(me), lanes(g)],
@@ -391,17 +420,17 @@
         )
 
     def relay_copy(part, d):
-        block = wide.at[part, half_rows(lax.rem(me + spans - d, spans))]
+        block = wide.at[part, half_rows(source(d))]
         return remote(block, block, relay_sem.at[part, d - 1], relay_leave.at[part], grp=1 - side)
 
     def weight_wait(part, d):
-        block = wide.at[part, half_rows(lax.rem(me + spans - d, spans))]
+        block = wide.at[part, half_rows(source(d))]
         sem = w_sem.at[part, d - 1]
-        return remote(block, block, sem, w_leave.at[leave_at(part, d)], sp=span_at(d))
+        return remote(block, block, sem, w_leave.at[leave_at(part, d)], sp=target(d))
 
     def when_extra(part, span, step):
-        if part == least:
-            pl.when(extra(span))(step)
+        if part >= least:
+            pl.when(holds(part, span))(step)
         else:
             step()
 
@@ -410,7 +439,7 @@
             for g in range(2):
                 weight_copy(part, d, g).start()
 
-        when_extra(part, span_at(d), step)
+        when_extra(part, target(d), step)
 
     def relay_weights(part, d):
         def step():
@@ -655,7 +684,7 @@
 
     def norm_hop(hop):
         for c in range(SLABS):
-            for way in range(2):
+            for way in WAYS:
 
                 @pl.when(inside(origin(way, hop)))
                 def _():
@@ -675,7 +704,7 @@
 
     with jax.named_scope("norm0"):
         for c in range(SLABS):
-            for way in range(2):
+            for way in WAYS:
                 spread_block(way, 0, c)
             cross_copy(me, c).start()
             mate_copy(me, c).start()
@@ -726,7 +755,7 @@
         )
 
     def has(part, span):
-        return inside(span) & extra(clamp(span)) if part == least else inside(span)
+        return inside(span) & holds(part, clamp(span)) if part >= least else inside(span)
 
     def hidden_start(part, way, hop, b):
         if hop + 1 >= spans:
@@ -737,7 +766,7 @@
             hidden_copy(part, way, hop, b).start()
 
     def hidden_pass(part, hop, b):
-        for way in range(2):
+        for way in WAYS:
 
             @pl.when(has(part, origin(way, hop)))
             def _():
@@ -747,16 +776,16 @@
 
     def make_hidden(part):
         twin_wait(part)
-        if part == least:
-
-            @pl.when(extra(me))
+        if part >= least:
+
+            @pl.when(holds(part, me))
             def _():
                 compute_hidden(part)
 
         else:
             compute_hidden(part)
         for b in range(blocks(part)):
-            for way in range(2):
+            for way in WAYS:
                 hidden_start(part, way, 0, b)
 
     pairs, crossing = {}, {}
@@ -826,7 +855,17 @@
             def _():
                 row_recv[me] = row_send[b]
 
+    inner_span = (me > 0) & (me < spans - 1)
+
+    def on_ends(part, d):
+        pl.when(jnp.logical_not(inner_span))(lambda: relay_weights(part, d))
+
+    def on_inner(part, d):
+        pl.when(inner_span)(lambda: relay_weights(part, d))
+
     actions = {
+        "e": on_ends,
+        "i": on_inner,
         "n": norm_hop,
         "x": cross_hop,
         "w": start_weights,
@@ -859,12 +898,12 @@
                 remote(
                     block, block, w_sem.at[part, 0], w_leave.at[part], sp=span_at(1)
                 ).wait_send()
-            for d in range(1, spans if part == least else 1):
+            for d in range(1, spans if part >= least else 1):
 
                 def sent():
                     weight_wait(part, d).wait_send()
 
-                when_extra(part, span_at(d), sent)
+                when_extra(part, target(d), sent)
 
             def relayed():
                 block = wide.at[part, pl.ds(0, (spans - 1) * half)]
@@ -933,8 +972,8 @@
     units = gate_weight.shape[1]
     part_cols, share = (model // spans, rows // shares)
     total = spans * rows
-    least, rest = tile_split(units // 128, spans)
-    parts = least + (rest > 0)
+    counts = tile_counts(units // 128, spans)
+    least, parts = min(counts[0]), max(counts[0])
     lines = log_decay.shape[0] * log_decay.shape[1]
     heads = width // HEAD
     rates = log_decay.reshape(lines, rows)
@@ -981,7 +1020,7 @@
             dma((2,)),
             dma((parts, spans - 1)),
             dma((parts, spans - 1)),
-            dma((least + spans - 1,)),
+            dma((least + (parts - least) * (spans - 1),)),
             dma((parts,)),
             dma((3, 2)),
             dma((2, spans - 1, SLABS)),

time: 84.1 us -> 83.1 us (0.988)
  Pallas kernels: 83.3 us -> 82.3 us
    pallas_call x1, Pallas kernels: 83.3 us -> 82.3 us  [fused_block(): pl.pallas_call(functools.partial(block_kernel, spans, shares), out_shape=...]
where the time goes in v4:
time: 83.1 us; the launch traced here: 82.9 us
  Pallas kernels  82.3 us (99%)
    pallas_call x1, Pallas kernels, fused_block(): pl.pallas_call(functools.partial(block_kernel, spans, shares), out_shape=...  82.3 us

profile of v4, /device:TPU:0, one launch (start us, length us, event | category | flops | bytes accessed | tf_op | source)
XLA Modules:
  0.0 82.9 jit_solution(3773708385509343956)
XLA Ops:
  0.0 82.3 %shard_map.136 = bf16[32,2048]{1,0:T(8,128)(2,1)S(1)} custom-call(bf16[128,256]{1,0:T(8,128)(2,1)} %query_hbm.1, bf16[128,256]{1,0:T(8,128)(2,1)} %key_hbm.1, bf16[128,256]{1,0:T(8,128)(2,1)} %value_hbm.1, bf16[128,256]{1,0:T(8,128)(2,1)} %gate_hbm.1, f32[4,128]{1,0:T(4,128)} %bitcast.3, f32[2,256]{1,0:T(2,128)} %gains_hbm.1, ...), custom_call_target="tpu_custom_call" | custom-call | tf_op jit(solution)/shard_map/pallas_call | solution.py:984
  82.3 0.7 copy.16

commit v5 on v4

--- a/solution.py
+++ b/solution.py
@@ -16,7 +16,8 @@
 WAYS = (0, 1)
 EARLY = ((0, 3), (0, 1), (0, 2))
 SECOND = ()
-ORDER = (('r', 0, 1), ('n', 1), ('x', 0), ('r', 0, 2), ('n', 2), ('w', 1, 1), ('x', 1), ('r', 0, 3), ('w', 1, 2), ('w', 1, 3), ('n', 3), ('x', 2), ('r', 1, 1), ('x', 3), ('m',), ('H', 0), ('w', 2, 1), ('r', 1, 3), ('w', 2, 2), ('r', 1, 2), ('w', 2, 3), ('h', 0, 1, 0), ('h', 0, 1, 1), ('H', 1), ('r', 2, 1), ('r', 2, 2), ('r', 2, 3), ('h', 0, 2, 0), ('h', 0, 2, 1), ('h', 0, 3, 0), ('h', 0, 3, 1), ('h', 1, 1, 0), ('h', 1, 1, 1), ('H', 2), ('h', 1, 2, 0), ('h', 1, 2, 1), ('h', 1, 3, 0), ('h', 1, 3, 1), ('h', 2, 1, 0), ('h', 2, 2, 0), ('h', 2, 3, 0), ('D', 0), ('h', 2, 1, 1), ('P', 0), ('h', 2, 2, 1), ('h', 2, 3, 1), ('D', 1), ('R', 0), ('P', 1), ('R', 1))
+ORDER = (('r', 0, 1), ('n', 1), ('x', 0), ('r', 0, 2), ('n', 2), ('w', 1, 1), ('x', 1), ('r', 0, 3), ('w', 1, 2), ('w', 1, 3), ('n', 3), ('x', 2), ('r', 1, 1), ('x', 3), ('m',), ('H', 0), ('w', 2, 1), ('r', 1, 3), ('w', 2, 2), ('r', 1, 2), ('w', 2, 3), ('h', 0, 1, 0), ('h', 0, 1, 1), ('H', 1), ('r', 2, 1), ('r', 2, 2), ('r', 2, 3), ('h', 0, 2, 0), ('h', 0, 2, 1), ('h', 1, 1, 0), ('h', 1, 1, 1), ('H', 2), ('h', 0, 3, 0), ('h', 0, 3, 1), ('h', 1, 2, 0), ('h', 1, 3, 0), ('h', 2, 1, 0), ('h', 2, 2, 0), ('h', 2, 3, 0), ('D', 0), ('h', 1, 2, 1), ('h', 1, 3, 1), ('h', 2, 1, 1), ('P', 0), ('h', 2, 2, 1), ('h', 2, 3, 1), ('D', 1), ('P', 1), ('R', 0), ('R', 1))
+EDGE = 16
 
 
 FULL_PRECISION = lax.Precision.HIGHEST
@@ -713,8 +714,6 @@
         for i in range(2):
             remote(whole, whole, gather_sem.at[i], leave_sem.at[0], tp=mate).wait_recv()
 
-    row_at = lax.broadcasted_iota(jnp.int32, (total, 1), 0)
-
     def twin_wait(part):
         def step():
             own_wait(part).wait()
@@ -723,25 +722,35 @@
 
         when_extra(part, me, step)
 
-    def compute_hidden(part):
+    groups = max(spans // 2, 1)
+    depth = spans // groups
+
+    def blocks(part):
+        return groups
+
+    def compute_hidden(part, b):
         cols = cols_of(part, me)
-        both = jnp.dot(norm_all[...], wide[part], preferred_element_type=f32)
+        size = total // groups
+        first, stop = b * size, (b + 1) * size
+        begin, end = max(first - EDGE, 0), min(stop + EDGE, total)
+        both = jnp.dot(norm_all[begin:end, :], wide[part], preferred_element_type=f32)
         here = both.astype(bf16).astype(f32)
-        earlier, later = pltpu.roll(here, 1, 0), pltpu.roll(here, total - 1, 0)
-        earlier = jnp.where(row_at == 0, 0.0, earlier)
-        later = jnp.where(row_at == total - 1, 0.0, later)
+        length = end - begin
+        row_at = lax.broadcasted_iota(jnp.int32, (length, 1), 0)
+        earlier, later = pltpu.roll(here, 1, 0), pltpu.roll(here, length - 1, 0)
+        if begin == 0:
+            earlier = jnp.where(row_at == 0, 0.0, earlier)
+        if end == total:
+            later = jnp.where(row_at == length - 1, 0.0, later)
         weight = jnp.concatenate(
             [gate_taps[:, cols].astype(f32), up_taps[:, cols].astype(f32)], axis=1
         )
         conv = weight[0:1] * earlier + weight[1:2] * here + weight[2:3] * later
+        conv = conv[first - begin : stop - begin]
         level = conv[:, :128]
-        hid_all[:, cols] = ((level / (1.0 + jnp.exp(-level))) * conv[:, 128:]).astype(bf16)
-
-    groups = max(spans // 2, 1)
-    depth = spans // groups
-
-    def blocks(part):
-        return groups
+        hid_all[first:stop, cols] = ((level / (1.0 + jnp.exp(-level))) * conv[:, 128:]).astype(
+            bf16
+        )
 
     def hidden_copy(part, way, hop, b):
         size = total // blocks(part)
@@ -776,15 +785,15 @@
 
     def make_hidden(part):
         twin_wait(part)
-        if part >= least:
-
-            @pl.when(holds(part, me))
-            def _():
-                compute_hidden(part)
-
-        else:
-            compute_hidden(part)
         for b in range(blocks(part)):
+            if part >= least:
+
+                @pl.when(holds(part, me))
+                def _():
+                    compute_hidden(part, b)
+
+            else:
+                compute_hidden(part, b)
             for way in WAYS:
                 hidden_start(part, way, 0, b)
 

time: 83.1 us -> 81.6 us (0.982)
  Pallas kernels: 82.3 us -> 80.8 us
    pallas_call x1, Pallas kernels: 82.3 us -> 80.8 us  [fused_block(): pl.pallas_call(functools.partial(block_kernel, spans, shares), out_shape=...]
where the time goes in v5:
time: 81.6 us; the launch traced here: 81.5 us
  Pallas kernels  80.8 us (99%)
    pallas_call x1, Pallas kernels, fused_block(): pl.pallas_call(functools.partial(block_kernel, spans, shares), out_shape=...  80.8 us

profile of v5, /device:TPU:0, one launch (start us, length us, event | category | flops | bytes accessed | tf_op | source)
XLA Modules:
  0.0 81.5 jit_solution(11943652788309034200)
XLA Ops:
  0.0 80.8 %shard_map.136 = bf16[32,2048]{1,0:T(8,128)(2,1)S(1)} custom-call(bf16[128,256]{1,0:T(8,128)(2,1)} %query_hbm.1, bf16[128,256]{1,0:T(8,128)(2,1)} %key_hbm.1, bf16[128,256]{1,0:T(8,128)(2,1)} %value_hbm.1, bf16[128,256]{1,0:T(8,128)(2,1)} %gate_hbm.1, f32[4,128]{1,0:T(4,128)} %bitcast.3, f32[2,256]{1,0:T(2,128)} %gains_hbm.1, ...), custom_call_target="tpu_custom_call" | custom-call | tf_op jit(solution)/shard_map/pallas_call | solution.py:993
  80.8 0.7 copy.16

commit v6 on v5

--- a/solution.py
+++ b/solution.py
@@ -836,7 +836,6 @@
             tp_mid.at[few], tp_recv.at[2, few], tp_sem.at[b, 2], tp_leave.at[0], tp=cross
         )
         crossing[b].start()
-        pairs[b][1].wait_recv()
 
     def row_out(b):
         d = lax.rem(b - me + spans, spans)
@@ -849,6 +848,7 @@
         )
 
     def row_step(group):
+        pairs[group][1].wait_recv()
         crossing[group].wait_recv()
         for b in range(group * depth, (group + 1) * depth):
             summed = tp_send[b, share_rows(lane), :].astype(f32)

time: 81.6 us -> 81.6 us (level)
  no operation moved by 1% of the time
where the time goes in v6:
time: 81.6 us; the launch traced here: 81.5 us
  Pallas kernels  80.8 us (99%)
    pallas_call x1, Pallas kernels, fused_block(): pl.pallas_call(functools.partial(block_kernel, spans, shares), out_shape=...  80.8 us

profile of v6, /device:TPU:0, one launch (start us, length us, event | category | flops | bytes accessed | tf_op | source)
XLA Modules:
  0.0 81.5 jit_solution(12030569773245284043)
XLA Ops:
  0.0 80.8 %shard_map.136 = bf16[32,2048]{1,0:T(8,128)(2,1)S(1)} custom-call(bf16[128,256]{1,0:T(8,128)(2,1)} %query_hbm.1, bf16[128,256]{1,0:T(8,128)(2,1)} %key_hbm.1, bf16[128,256]{1,0:T(8,128)(2,1)} %value_hbm.1, bf16[128,256]{1,0:T(8,128)(2,1)} %gate_hbm.1, f32[4,128]{1,0:T(4,128)} %bitcast.3, f32[2,256]{1,0:T(2,128)} %gains_hbm.1, ...), custom_call_target="tpu_custom_call" | custom-call | tf_op jit(solution)/shard_map/pallas_call | solution.py:993
  80.8 0.7 copy.16
